TPU v7x, 512 devices: a whole 4x8x8 slice. The times are simulated.
512 devices in a mesh: fs: 64 (over z, y), tp: 8 (over x, core).
Axes of the slice: x: 4, y: 8, z: 8, core: 2. Of those that a mesh axis runs over, the one named last changes fastest.
Arguments:
- inputs: bfloat16 [32768, 2048], P('fs', 'tp'), may hold values from -6 to 6
- value_cotangent: bfloat16 [32768, 2048], P('fs', 'tp'), may hold values from -6 to 6
- first_map: bfloat16 [32768, 2048], P('fs', 'tp'), may hold values from -6 to 6
- second_map: bfloat16 [32768, 2048], P('fs', 'tp'), may hold values from -6 to 6
- lambdas: float32 [16], P('tp'), may hold values from 0.3 to 0.8
- head_gain: float32 [128], replicated, may hold values from 0.1 to 1.9
- output_cotangent: bfloat16 [32768, 2048], P('fs', 'tp'), may hold values from -6 to 6
- value_factor: bfloat16 [2048, 256], replicated, may hold values from -0.125 to 0.125
- output_factor: bfloat16 [2048, 256], replicated, may hold values from -0.125 to 0.125
- value_weight: float32 [2048, 2048], P('fs', 'tp'), may hold values from -0.125 to 0.125
- output_weight: float32 [2048, 2048], P('tp', 'fs'), may hold values from -0.125 to 0.125
- value_moment: float32 [256, 2048], P('fs', 'tp'), may hold values from -6 to 6
- value_second: float32 [256, 2048], P('fs', 'tp'), may hold values from 0.25 to 4
- output_moment: float32 [256, 2048], P('fs', 'tp'), may hold values from -6 to 6
- output_second: float32 [256, 2048], P('fs', 'tp'), may hold values from 0.25 to 4
Outputs:
- value_master: float32 [2048, 2048], P('fs', 'tp')
- output_master: float32 [2048, 2048], P('tp', 'fs')
- value_moment_new: float32 [256, 2048], P('fs', 'tp')
- value_second_new: float32 [256, 2048], P('fs', 'tp')
- output_moment_new: float32 [256, 2048], P('fs', 'tp')
- output_second_new: float32 [256, 2048], P('fs', 'tp')
- value_copy: bfloat16 [2048, 2048], P(None, 'tp')
- output_copy: bfloat16 [2048, 2048], P('tp')
All inputs are finite; a program needn't handle non-finite values.
Results may differ from a plain program's by a relative error of at most 0.0027.
Values may be sent and summed in bfloat16 or wider, within the bound.
A program may use at most 64 MiB of HBM per device.

v0:
```python
import math

import jax
import jax.numpy as jnp
from jax import lax
from jax.sharding import PartitionSpec as P


def side_by_side(arrays, axis, dim, along):
    ends, at = ([], 0)
    for a in arrays[:-1]:
        at += a.shape[along]
        ends.append(at)
    both = jnp.concatenate(arrays, axis=along)
    return tuple(jnp.split(lax.all_gather(both, axis, axis=dim, tiled=True), ends, axis=along))


def cut_along(x, dim, size):
    before, after = (x.shape[:dim], x.shape[dim + 1 :])
    return jnp.moveaxis(x.reshape(*before, size, -1, *after), dim, 0)


def sum_at_owner(x, axis, dim):
    size = lax.axis_size(axis)
    tiles = lax.all_to_all(cut_along(x, dim, size), axis, 0, 0, tiled=True)
    return jnp.sum(tiles.astype(jnp.float32), axis=0)


def laid_out(tiles, dim):
    tiles = jnp.moveaxis(tiles, 0, dim)
    lengths = tiles.shape
    return tiles.reshape(*lengths[:dim], lengths[dim] * lengths[dim + 1], *lengths[dim + 2 :])


def copy_for_each(x, axis):
    size = lax.axis_size(axis)
    return lax.all_to_all(jnp.broadcast_to(x[None], (size, *x.shape)), axis, 0, 0, tiled=True)


def gathered_copies(x, axis, dim):
    return laid_out(copy_for_each(x, axis), dim)


def gather_turned(arrays, axis, dims):
    turned = [jnp.moveaxis(a, dim, 0) for a, dim in zip(arrays, dims)]
    both = jnp.concatenate([t.reshape(len(t), -1) for t in turned], axis=1)
    filled, at, done = (lax.all_gather(both, axis, axis=0, tiled=True), 0, [])
    for t, dim in zip(turned, dims):
        slab = filled[:, at : at + t[0].size].reshape(-1, *t.shape[1:])
        done.append(jnp.moveaxis(slab, 0, dim))
        at += t[0].size
    return tuple(done)


def contract_rows(left, right, precise):
    if precise:
        return lax.dot_general(
            left,
            right,
            (((0,), (0,)), ((), ())),
            precision=lax.Precision.HIGHEST,
            preferred_element_type=jnp.float32,
        )
    return lax.dot_general(
        left, right, (((0,), (0,)), ((), ())), preferred_element_type=jnp.float32
    )


def local(
    inputs,
    value_cotangent,
    first_map,
    second_map,
    lambdas,
    head_gain,
    output_cotangent,
    value_factor,
    output_factor,
    value_weight,
    output_weight,
    value_moment,
    value_second,
    output_moment,
    output_second,
):
    tok_rows = inputs.shape[0]
    local_heads = lambdas.shape[0]
    head_width = head_gain.shape[0]
    head_cols = local_heads * head_width
    first = first_map.astype(jnp.float32).reshape(tok_rows, local_heads, head_width)
    second = second_map.astype(jnp.float32).reshape(tok_rows, local_heads, head_width)
    difference = first - lambdas[None, :, None] * second
    normed = (
        difference
        * lax.rsqrt(jnp.mean(difference * difference, axis=-1, keepdims=True) + 1e-06)
        * head_gain
    )
    heads_out = normed.reshape(tok_rows, head_cols).astype(jnp.bfloat16)
    full_inputs, full_cotangent = side_by_side((inputs, output_cotangent), "tp", 1, 0)
    token_scale = 1.0 / math.sqrt(tok_rows * lax.axis_size("fs"))
    fs_index = lax.axis_index("fs")
    width_rows = value_weight.shape[0]
    value_rows = lax.dynamic_slice_in_dim(
        value_factor, fs_index * width_rows, width_rows, 0
    ).astype(jnp.float32)
    output_rows = lax.dynamic_slice_in_dim(
        output_factor, fs_index * width_rows, width_rows, 0
    ).astype(jnp.float32)
    grad_value = contract_rows(full_inputs, value_cotangent, False) * token_scale
    grad_output = contract_rows(full_cotangent, heads_out, False) * token_scale
    partial_value = jnp.concatenate(
        [
            contract_rows(value_factor.astype(jnp.float32), grad_value, True),
            contract_rows(output_factor.astype(jnp.float32), grad_output, True),
        ],
        axis=1,
    )
    own_rows = sum_at_owner(partial_value.astype(jnp.bfloat16), "fs", 0)
    moments = jnp.concatenate([value_moment, output_moment], axis=1)
    seconds = jnp.concatenate([value_second, output_second], axis=1)
    moment_new = 0.8 * moments + 0.2 * own_rows
    second_new = 0.95 * seconds + 0.05 * own_rows * own_rows
    direction = moment_new / (jnp.sqrt(second_new) + 1e-08)
    full_direction = gathered_copies(direction, "fs", 0)
    step_value = jnp.dot(
        value_rows,
        full_direction[:, :head_cols],
        precision=lax.Precision.HIGHEST,
        preferred_element_type=jnp.float32,
    )
    step_output = jnp.dot(
        output_rows,
        full_direction[:, head_cols:],
        precision=lax.Precision.HIGHEST,
        preferred_element_type=jnp.float32,
    )
    value_master = value_weight - 0.05 * step_value
    output_master = output_weight - 0.05 * step_output.T
    value_copy, output_copy = gather_turned(
        (value_master.astype(jnp.bfloat16), output_master.astype(jnp.bfloat16)), "fs", (0, 1)
    )
    return (
        value_master,
        output_master,
        moment_new[:, :head_cols],
        second_new[:, :head_cols],
        moment_new[:, head_cols:],
        second_new[:, head_cols:],
        value_copy,
        output_copy,
    )


def solution(mesh):
    in_specs = (
        P("fs", "tp"),
        P("fs", "tp"),
        P("fs", "tp"),
        P("fs", "tp"),
        P("tp"),
        P(),
        P("fs", "tp"),
        P(),
        P(),
        P("fs", "tp"),
        P("tp", "fs"),
        P("fs", "tp"),
        P("fs", "tp"),
        P("fs", "tp"),
        P("fs", "tp"),
    )
    out_specs = (
        P("fs", "tp"),
        P("tp", "fs"),
        P("fs", "tp"),
        P("fs", "tp"),
        P("fs", "tp"),
        P("fs", "tp"),
        P(None, "tp"),
        P("tp", None),
    )
    return jax.shard_map(local, mesh=mesh, in_specs=in_specs, out_specs=out_specs, check_vma=False)
```

profile of v0, /device:TPU:6, one launch (start us, length us, event | category | flops | bytes accessed | tf_op | source)
XLA Modules:
  0.0 207.0 jit_solution(13290908280082833347)
XLA Ops:
  7.3 1.9 pad_maximum_fusion
  9.2 1.3 reshape.84
  10.5 0.3 reshape.85
  10.8 0.7 multiply_reduce_fusion
  11.6 43.9 %all-gather.3.cloned.1.call-done = bf16[1024,2048]{1,0:T(8,128)(2,1)} async-done(((bf16[1024,256]{1,0:T(8,128)(2,1)}), bf16[1024,2048]{1,0:T(8,128)(2,1)}) %all-gather.3.cloned.1.call-update) | async-done | bytes 4194320 | tf_op jit(solution)/shard_map/all_gather | solution.py:15
  55.5 0.6 mul.124
  56.2 2.5 %convolution_multiply_fusion = f32[2048,256]{1,0:T(8,128)S(1)} fusion(bf16[1024,2048]{1,0:T(8,128)(2,1)} %all-gather.3.cloned.1.call-done, f32[64,8,2,128]{3,2,1,0:T(2,128)S(1)} %bitcast.25, f32[256]{0:T(256)S(1)} %get-tuple-element.43, f32[256]{0:T(256)S(1)} %get-tuple-element.44, bf16[512,256]{1,0:T(8,128)(2,1)S(1)} %copy-done.3, ...), kind=kOutput, calls=%fused_computation | convolution fusion | flops 538312704 | bytes 5244928 | tf_op jit(solution)/shard_map/dot_general | solution.py:64
  58.7 1.5 fusion.3
  60.3 2.3 %convolution_multiply_fusion.1 = f32[2048,256]{1,0:T(8,128)S(1)} fusion(bf16[512,256]{1,0:T(8,128)(2,1)S(1)} %copy-done.13, bf16[1024,2048]{1,0:T(8,128)(2,1)} %all-gather.3.cloned.1.call-done), kind=kOutput, calls=%fused_computation.1 | convolution fusion | flops 537395200 | bytes 4456448 | tf_op jit(solution)/shard_map/dot_general | solution.py:64
  62.7 1.5 fusion.2
  64.4 28.4 %all_to_all.10 = bf16[64,4,512]{2,1,0:T(4,128)(2,1)S(1)} all-to-all(bf16[64,4,512]{2,1,0:T(4,128)(2,1)S(1)} %pad_maximum_fusion.1), channel_id=1, replica_groups=mesh['fs'=64,'tp'=8] {'fs'}, dimensions={0} | all-to-all | bytes 524288 | tf_op jit(solution)/shard_map/all_to_all | solution.py:25
  92.8 0.1 convert_reduce_fusion
  93.0 0.9 broadcast_in_dim.2
  93.8 4.6 %all-to-all-start.1 = ((f32[64,4,512]{2,1,0:T(4,128)}), f32[64,4,512]{2,1,0:T(4,128)S(1)}, u32[]{:S(2)}, u32[]{:S(2)}) async-start(f32[64,4,512]{2,1,0:T(4,128)} %broadcast_in_dim.2), calls=%async_computation.1 | async-start | bytes 1048576 | tf_op jit(solution)/shard_map/all_to_all | solution.py:37
  98.5 18.6 %all-to-all-done.1 = f32[64,4,512]{2,1,0:T(4,128)S(1)} async-done(((f32[64,4,512]{2,1,0:T(4,128)}), f32[64,4,512]{2,1,0:T(4,128)S(1)}, u32[]{:S(2)}, u32[]{:S(2)}) %all-to-all-start.1) | async-done | bytes 524320 | tf_op jit(solution)/shard_map/all_to_all | solution.py:37
  117.1 0.2 reshape.86
  117.3 0.2 fusion.4
  117.6 0.9 fusion.25
  118.5 0.6 pad_maximum_fusion.2
  119.1 0.6 fusion.23
  119.7 0.6 fusion.24
  120.3 75.8 %all-gather.5.cloned.1.call-done = bf16[2048,512]{1,0:T(8,128)(2,1)} async-done(((bf16[32,512]{1,0:T(8,128)(2,1)}), bf16[2048,512]{1,0:T(8,128)(2,1)}) %all-gather.5.cloned.1.call-update) | async-done | bytes 2097168 | tf_op jit(solution)/shard_map/all_gather | solution.py:47
  196.1 2.6 %slice_bitcast_fusion = (bf16[256,2048]{0,1:T(8,128)(2,1)S(1)}, bf16[2048,256]{1,0:T(8,128)(2,1)}) fusion(bf16[2048,512]{1,0:T(8,128)(2,1)} %all-gather.5.cloned.1.call-done), kind=kLoop, calls=%fused_computation.12 | loop fusion | bytes 4194304 | tf_op jit(solution)/shard_map/transpose | solution.py:50
  198.7 1.4 copy.28
  (39 shorter events, 0.5 us)
Async XLA Ops:
  7.2 55.4 %copy-start = (bf16[2048,256]{1,0:T(8,128)(2,1)S(1)}, bf16[2048,256]{1,0:T(8,128)(2,1)}, u32[]{:S(2)}) copy-start(bf16[2048,256]{1,0:T(8,128)(2,1)} %param.22) | copy-start | bytes 3145732
  7.2 3.3 %copy-start.3 = (bf16[512,256]{1,0:T(8,128)(2,1)S(1)}, bf16[512,256]{1,0:T(8,128)(2,1)}, u32[]{:S(2)}) copy-start(bf16[512,256]{1,0:T(8,128)(2,1)} %param.18) | copy-start | bytes 786436
  7.2 3.6 %copy-start.11 = (f32[2]{0:T(128)S(1)}, f32[2]{0:T(128)}, u32[]{:S(2)}) copy-start(f32[2]{0:T(128)} %param.19) | copy-start | bytes 28
  7.2 4.3 %copy-start.12 = (f32[128]{0:T(128)S(1)}, f32[128]{0:T(128)}, u32[]{:S(2)}) copy-start(f32[128]{0:T(128)} %param.20) | copy-start | bytes 1540
  7.2 48.3 %all-gather.3.cloned.1.call-start = ((), (), s32[]{:S(2)}) async-start(), calls=%async_computation.2 | async-start | bytes 4718592 | tf_op jit(solution)/shard_map/all_gather | solution.py:15
  9.2 46.9 %copy-start.2 = (bf16[512,256]{1,0:T(8,128)(2,1)S(1)}, bf16[512,256]{1,0:T(8,128)(2,1)}, u32[]{:S(2)}) copy-start(bf16[512,256]{1,0:T(8,128)(2,1)} %param.17) | copy-start | bytes 786436
  56.1 2.5 %copy-start.1 = (bf16[2048,256]{1,0:T(8,128)(2,1)S(1)}, bf16[2048,256]{1,0:T(8,128)(2,1)}, u32[]{:S(2)}) copy-start(bf16[2048,256]{1,0:T(8,128)(2,1)} %param.23) | copy-start | bytes 3145732
  58.7 1.6 copy-start.13
  62.6 30.3 %copy-start.7 = (f32[4,256]{1,0:T(4,128)S(1)}, f32[4,256]{1,0:T(4,128)}, u32[]{:S(2)}) copy-start(f32[4,256]{1,0:T(4,128)} %param.29) | copy-start | bytes 12292
  62.6 30.3 %copy-start.8 = (f32[4,256]{1,0:T(4,128)S(1)}, f32[4,256]{1,0:T(4,128)}, u32[]{:S(2)}) copy-start(f32[4,256]{1,0:T(4,128)} %param.27) | copy-start | bytes 12292
  62.6 30.3 %copy-start.9 = (f32[4,256]{1,0:T(4,128)S(1)}, f32[4,256]{1,0:T(4,128)}, u32[]{:S(2)}) copy-start(f32[4,256]{1,0:T(4,128)} %param.28) | copy-start | bytes 12292
  62.6 30.3 %copy-start.10 = (f32[4,256]{1,0:T(4,128)S(1)}, f32[4,256]{1,0:T(4,128)}, u32[]{:S(2)}) copy-start(f32[4,256]{1,0:T(4,128)} %param.26) | copy-start | bytes 12292
  64.2 53.2 %copy-start.5 = (f32[256,32]{0,1:T(8,128)S(1)}, f32[256,32]{0,1:T(8,128)}, u32[]{:S(2)}) copy-start(f32[256,32]{0,1:T(8,128)} %param.25) | copy-start | bytes 98308
  64.2 53.4 %copy-start.6 = (f32[32,256]{1,0:T(8,128)S(1)}, f32[32,256]{1,0:T(8,128)}, u32[]{:S(2)}) copy-start(f32[32,256]{1,0:T(8,128)} %param.24) | copy-start | bytes 98308
  93.8 23.3 %all-to-all-start.1 = ((f32[64,4,512]{2,1,0:T(4,128)}), f32[64,4,512]{2,1,0:T(4,128)S(1)}, u32[]{:S(2)}, u32[]{:S(2)}) async-start(f32[64,4,512]{2,1,0:T(4,128)} %broadcast_in_dim.2), calls=%async_computation.1 | async-start | bytes 1048576 | tf_op jit(solution)/shard_map/all_to_all | solution.py:37
  98.5 97.6 %all-gather.5.cloned.1.call-start = ((), (), s32[]{:S(2)}) async-start(), calls=%async_computation.3 | async-start | bytes 2129920 | tf_op jit(solution)/shard_map/all_gather | solution.py:47
  117.6 81.2 %copy-start.4 = (f32[256,32]{0,1:T(8,128)}, f32[256,32]{0,1:T(8,128)S(1)}, u32[]{:S(2)}) copy-start(f32[256,32]{0,1:T(8,128)S(1)} %fusion.4) | copy-start | bytes 98308
Sparse Core Ops, SparseCore 0:
  10.7 44.7 all-gather.2
  119.2 76.8 all-gather.4
where the time goes:
time: 207 us
  waiting for transfers between devices  138 us (67%)
  blocking collectives  28.4 us (14%)
  between operations  14.3 us (7%)
  matrix products  8.93 us (4%)
  local copies, waits for them, and re-layouts  8.65 us (4%)
  starting transfers between devices  4.71 us (2%)
  other arithmetic  3.6 us (2%)
    all_gather x1, waiting for transfers between devices, gather_turned(): filled, at, done = (lax.all_gather(both, axis, axis=0, tiled=True), 0, [])  75.8 us
    all_gather x1, waiting for transfers between devices, side_by_side(): lax.all_gather(both, axis, axis=dim, tiled=True)  43.9 us
    all_to_all x1, blocking collectives, sum_at_owner(): tiles = lax.all_to_all(cut_along(x, dim, size), axis, 0, 0, tiled=True)  28.4 us
    all_to_all x1, waiting for transfers between devices, copy_for_each(): lax.all_to_all(jnp.broadcast_to(x[None], (size, *x.shape)), axis, 0, 0, t...  18.6 us
    dot_general x2, matrix products, contract_rows(): lax.dot_general(left, right, (((0,), (0,)), ((), ())), preferred_element_...  4.84 us
    all_to_all x1, starting transfers between devices, copy_for_each(): lax.all_to_all(jnp.broadcast_to(x[None], (size, *x.shape)), axis, 0, 0, t...  4.63 us
  transfers between devices with their start and end apart: 3, of which 3 were waited for; matrix products, arithmetic and copies ran while one was open for 2% of the time, Pallas kernels for 0%

commit v1 on v0

v1 whole, which is shorter than its diff:
```python
import functools
import math

import jax
import jax.numpy as jnp
from jax import lax
from jax.experimental import pallas as pl
from jax.experimental.pallas import tpu as pltpu
from jax.sharding import PartitionSpec as P

MESH = pl.DeviceIdType.MESH
X, C, Y, Z = 4, 2, 8, 8
F32, BF16 = jnp.float32, jnp.bfloat16
RANK, HEAD = 256, 128
WIDTH_ROWS = 32
WEIGHT_RATE = 960.0
DIRECTION_RATE = 11.0


def encode(value, rate):
    size = jnp.exp2(jnp.abs(value) * rate) - 1.0
    return jnp.where(value < 0, -size, size).astype(BF16)


def decode(code, rate):
    code = code.astype(F32)
    size = jnp.log(1.0 + jnp.abs(code)) * (1.0 / (rate * math.log(2.0)))
    return jnp.where(code < 0, -size, size)


def rows_dot(left, right):
    return lax.dot_general(left, right, (((0,), (0,)), ((), ())), preferred_element_type=F32)


def exchange_kernel(
    inputs, ocot, vcot, first, second, lambdas, gain, vf, of, vw, ow, vm, vs, om, os_,
    wv_out, wo_out, da_out, db_out, low_out,
    in_v, oc_v, vc_v, fi_v, se_v, vf_v, of_v, vw_v, ow_v, mom_v, sec_v,
    pair, ax, sx, rx, pq, heads,
    la, lb, ra, rb, sa, sb, ra2, rb2, da, db, wv, wo, low_v,
    load_sem, out_sem,
    pair_s, pair_r, xs_s, xs_r, xg_s, xg_r, fw_s, fw_r,
    r1a_s, r1a_r, r1b_s, r1b_r, r2a_s, r2a_r, r2b_s, r2b_r,
    g1a_s, g1a_r, g1b_s, g1b_r, g2a_s, g2a_r, g2b_s, g2b_r,
    w1v_s, w1v_r, w1o_s, w1o_r, wrv_s, wrv_r, wro_s, wro_r,
):
    fs = lax.axis_index("fs")
    tp = lax.axis_index("tp")
    z, y = fs // Y, lax.rem(fs, Y)
    x, c = tp // C, lax.rem(tp, C)

    def at_x(d):
        return (fs, lax.rem(x + d, X) * C + c)

    def at_y(d):
        return (z * Y + lax.rem(y + d, Y), tp)

    def at_z(d):
        return (lax.rem(z + d, Z) * Y + y, tp)

    partner = (fs, x * C + (1 - c))

    def send(src, dst, s, r, where):
        copy = pltpu.make_async_remote_copy(
            src_ref=src, dst_ref=dst, send_sem=s, recv_sem=r, device_id=where, device_id_type=MESH
        )
        copy.start()
        return copy

    chip_rows = pl.ds(pl.multiple_of(x * (C * 256), C * 256), C * 256)
    loads = {}
    for i, (name, src, dst) in enumerate(
        [
            ("vw", vw, vw_v),
            ("ow", ow, ow_v),
            ("in", inputs, in_v),
            ("oc", ocot, oc_v),
            ("vf", vf.at[chip_rows], vf_v),
            ("of", of.at[chip_rows], of_v),
            ("fi", first, fi_v),
            ("se", second, se_v),
            ("vc", vcot, vc_v),
            ("vm", vm, mom_v.at[pl.ds(0, 4)]),
            ("om", om, mom_v.at[pl.ds(4, 4)]),
            ("vs", vs, sec_v.at[pl.ds(0, 4)]),
            ("os", os_, sec_v.at[pl.ds(4, 4)]),
        ]
    ):
        loads[name] = pltpu.make_async_copy(src, dst, load_sem.at[i])
        loads[name].start()

    barrier = pltpu.get_barrier_semaphore()
    friends = (
        [partner]
        + [at_x(d) for d in range(1, X)]
        + [at_y(d) for d in range(1, Y)]
        + [at_z(d) for d in range(1, Z)]
    )
    for friend in friends:
        pl.semaphore_signal(barrier, inc=1, device_id=friend, device_id_type=MESH)

    loads["vw"].wait()
    wv[z, y] = encode(vw_v[...], WEIGHT_RATE)
    loads["ow"].wait()
    turned = jnp.concatenate([ow_v[...], jnp.zeros((256, 128 - WIDTH_ROWS), F32)], axis=1).T
    wo[z, y] = encode(turned[:WIDTH_ROWS], WEIGHT_RATE)
    loads["in"].wait()
    loads["oc"].wait()
    loads["vf"].wait()
    loads["of"].wait()
    pl.semaphore_wait(barrier, len(friends))

    mine = pl.ds(pl.multiple_of(c * 256, 256), 256)
    theirs = pl.ds(pl.multiple_of((1 - c) * 256, 256), 256)
    to_pair = [
        send(in_v.at[theirs], pair.at[0], pair_s.at[0], pair_r.at[0], partner),
        send(oc_v.at[theirs], pair.at[1], pair_s.at[1], pair_r.at[1], partner),
    ]
    w1v = [
        send(wv.at[z, y], wv.at[z, y], w1v_s.at[d], w1v_r.at[d], at_y(d)) for d in range(1, Y)
    ]
    w1o = [
        send(wo.at[z, y], wo.at[z, y], w1o_s.at[d], w1o_r.at[d], at_z(d)) for d in range(1, Z)
    ]
    acc_p = jnp.dot(in_v[mine], vf_v[mine], preferred_element_type=F32)
    acc_q = jnp.dot(oc_v[mine], of_v[mine], preferred_element_type=F32)
    for copy in to_pair:
        copy.wait_recv()
    acc_p += jnp.dot(pair[0], vf_v[theirs], preferred_element_type=F32)
    acc_q += jnp.dot(pair[1], of_v[theirs], preferred_element_type=F32)
    acc = jnp.concatenate([acc_p, acc_q], axis=1).reshape(X, 64, 512)
    ax[...] = acc
    sx[...] = acc.astype(BF16)
    x_sum = [
        send(sx.at[lax.rem(x + d, X)], rx.at[x], xs_s.at[d], xs_r.at[d], at_x(d))
        for d in range(1, X)
    ]

    loads["fi"].wait()
    loads["se"].wait()
    for h in range(2):
        cols = slice(h * HEAD, (h + 1) * HEAD)
        difference = fi_v[:, cols].astype(F32) - lambdas[h] * se_v[:, cols].astype(F32)
        mean = jnp.mean(difference * difference, axis=-1, keepdims=True)
        heads[:, cols] = (difference * lax.rsqrt(mean + 1e-06) * gain[...]).astype(BF16)

    total = ax[x]
    for d, copy in zip(range(1, X), x_sum):
        copy.wait_recv()
        total += rx[lax.rem(x + X - d, X)].astype(F32)
    pq[c, x] = total.astype(BF16)
    x_all = [
        send(pq.at[c, x], pq.at[c, x], xg_s.at[d], xg_r.at[d], at_x(d)) for d in range(1, X)
    ]
    passed = [send(pq.at[c, x], pq.at[c, x], fw_s.at[0], fw_r.at[0], partner)]

    for copy in w1v + w1o:
        copy.wait_recv()

    def ring_step(s):
        out = []
        zr, yr = lax.rem(z + Z - (s - 1), Z), lax.rem(y + Y - (s - 1), Y)
        zl, yl = lax.rem(z + (s - 1), Z), lax.rem(y + (s - 1), Y)
        out.append(send(wv.at[zr], wv.at[zr], wrv_s.at[s], wrv_r.at[s], at_z(1)))
        out.append(
            send(wo.at[:, pl.ds(yr, 1)], wo.at[:, pl.ds(yr, 1)], wro_s.at[s], wro_r.at[s], at_y(1))
        )
        if s < 4:
            k = 4 + s
            out.append(send(wv.at[zl], wv.at[zl], wrv_s.at[k], wrv_r.at[k], at_z(Z - 1)))
            out.append(
                send(
                    wo.at[:, pl.ds(yl, 1)], wo.at[:, pl.ds(yl, 1)], wro_s.at[k], wro_r.at[k],
                    at_y(Y - 1),
                )
            )
        return out

    rings = [ring_step(1)]

    for d, copy in zip(range(1, X), x_all):
        copy.wait_recv()
        xx = lax.rem(x + X - d, X)
        passed.append(send(pq.at[c, xx], pq.at[c, xx], fw_s.at[d], fw_r.at[d], partner))
    loads["vc"].wait()
    pq_mine = pq[c].reshape(256, 512)
    lv = rows_dot(pq_mine[:, :RANK], vc_v[mine])
    lo = rows_dot(pq_mine[:, RANK:], heads[mine])
    for copy in passed:
        copy.wait_recv()
    pq_theirs = pq[1 - c].reshape(256, 512)
    lv += rows_dot(pq_theirs[:, :RANK], vc_v[theirs])
    lo += rows_dot(pq_theirs[:, RANK:], heads[theirs])
    scale = 1.0 / math.sqrt(32768.0)
    lv3 = (lv * scale).reshape(32, 8, 256)
    lo3 = (lo * scale).reshape(32, 8, 256)
    upper = lax.broadcasted_iota(jnp.int32, (32, 8, 256), 1) < 4
    even = jnp.where(upper, lv3, pltpu.roll(lo3, 4, 1)).astype(BF16)
    odd = jnp.where(upper, pltpu.roll(lv3, 4, 1), lo3).astype(BF16)
    for f in range(Z * Y):
        block = (odd if f % 2 else even)[f // 2]
        la[f // Y, f % Y] = block[:, :128]
        lb[f % Y, f // Y] = block[:, 128:]
    r1a = [
        send(la.at[lax.rem(z + d, Z)], ra.at[z], r1a_s.at[d], r1a_r.at[d], at_z(d))
        for d in range(1, Z)
    ]
    r1b = [
        send(lb.at[lax.rem(y + d, Y)], rb.at[y], r1b_s.at[d], r1b_r.at[d], at_y(d))
        for d in range(1, Y)
    ]

    for copy in rings[0]:
        copy.wait_recv()
    rings.append(ring_step(2))

    sum_a = la[z].astype(F32)
    sum_b = lb[y].astype(F32)
    for d in range(1, 8):
        r1a[d - 1].wait_recv()
        sum_a += ra[lax.rem(z + Z - d, Z)].astype(F32)
        r1b[d - 1].wait_recv()
        sum_b += rb[lax.rem(y + Y - d, Y)].astype(F32)
    sa[...] = sum_a
    sb[...] = sum_b
    r2a = [
        send(sa.at[lax.rem(y + d, Y)], ra2.at[y], r2a_s.at[d], r2a_r.at[d], at_y(d))
        for d in range(1, Y)
    ]
    r2b = [
        send(sb.at[lax.rem(z + d, Z)], rb2.at[z], r2b_s.at[d], r2b_r.at[d], at_z(d))
        for d in range(1, Z)
    ]

    for copy in rings[1]:
        copy.wait_recv()
    rings.append(ring_step(3))

    low_a = sa[y]
    low_b = sb[z]
    for d in range(1, 8):
        r2a[d - 1].wait_recv()
        low_a += ra2[lax.rem(y + Y - d, Y)]
        r2b[d - 1].wait_recv()
        low_b += rb2[lax.rem(z + Z - d, Z)]
    low = jnp.concatenate([low_a, low_b], axis=1)
    low_v[...] = low
    for name in ("vm", "om", "vs", "os"):
        loads[name].wait()
    moment = 0.8 * mom_v[...] + 0.2 * low
    spread = 0.95 * sec_v[...] + 0.05 * low * low
    code = encode(moment / (jnp.sqrt(spread) + 1e-08), DIRECTION_RATE)
    da[z, y] = code[:, :128]
    db[y, z] = code[:, 128:]
    g1a = [
        send(da.at[z, y], da.at[z, y], g1a_s.at[d], g1a_r.at[d], at_y(d)) for d in range(1, Y)
    ]
    g1b = [
        send(db.at[y, z], db.at[y, z], g1b_s.at[d], g1b_r.at[d], at_z(d)) for d in range(1, Z)
    ]

    for copy in rings[2]:
        copy.wait_recv()
    rings.append(ring_step(4))

    for copy in g1a:
        copy.wait_recv()
    g2a = [send(da.at[z], da.at[z], g2a_s.at[d], g2a_r.at[d], at_z(d)) for d in range(1, Z)]
    for copy in g1b:
        copy.wait_recv()
    g2b = [send(db.at[y], db.at[y], g2b_s.at[d], g2b_r.at[d], at_y(d)) for d in range(1, Y)]

    for copy in rings[3]:
        copy.wait_recv()
    outs = [
        pltpu.make_async_copy(wv, wv_out, out_sem.at[0]),
        pltpu.make_async_copy(wo, wo_out, out_sem.at[1]),
        pltpu.make_async_copy(low_v, low_out, out_sem.at[2]),
    ]
    for copy in outs:
        copy.start()
    for copy in g2a + g2b:
        copy.wait_recv()
    last = [
        pltpu.make_async_copy(da, da_out, out_sem.at[3]),
        pltpu.make_async_copy(db, db_out, out_sem.at[4]),
    ]
    for copy in last:
        copy.start()
    sent = to_pair + w1v + w1o + x_sum + x_all + passed + r1a + r1b + r2a + r2b
    sent += g1a + g1b + g2a + g2b
    for ring in rings:
        sent += ring
    for copy in sent:
        copy.wait_send()
    for copy in outs + last:
        copy.wait()


def finish_kernel(
    da, db, wv, wo, vf, of, low, vw, ow, vm, vs, om, os_,
    vmaster, omaster, vm_new, vs_new, om_new, os_new, vcopy, ocopy,
    dv_hi, dv_lo, do_hi, do_lo, sv, so, turn,
):
    j = pl.program_id(0)
    fs = lax.axis_index("fs")

    @pl.when(j == 0)
    def _():
        low_v, low_o = low[0:4], low[4:8]
        vm_new[...] = 0.8 * vm[...] + 0.2 * low_v
        vs_new[...] = 0.95 * vs[...] + 0.05 * low_v * low_v
        om_new[...] = 0.8 * om[...] + 0.2 * low_o
        os_new[...] = 0.95 * os_[...] + 0.05 * low_o * low_o
        upper = lax.broadcasted_iota(jnp.int32, (8, 256), 0) < 4
        for g in range(Z * Y // 2):
            zz, yy = (2 * g) // Y, (2 * g) % Y
            even = decode(jnp.concatenate([da[zz, yy], db[yy, zz]], axis=1), DIRECTION_RATE)
            odd = decode(
                jnp.concatenate([da[zz, yy + 1], db[yy + 1, zz]], axis=1), DIRECTION_RATE
            )
            value = jnp.where(upper, even, pltpu.roll(odd, 4, 0))
            output = jnp.where(upper, pltpu.roll(even, 4, 0), odd)
            rows = slice(8 * g, 8 * g + 8)
            for full, hi, lo in ((value, dv_hi, dv_lo), (output, do_hi, do_lo)):
                top = full.astype(BF16)
                hi[rows] = top
                lo[rows] = (full - top.astype(F32)).astype(BF16)

    def step(factor, hi, lo):
        out = jnp.dot(factor[...], hi[...], preferred_element_type=F32)
        return 0.05 * (out + jnp.dot(factor[...], lo[...], preferred_element_type=F32))

    sv[...] = step(vf, dv_hi, dv_lo)
    so[...] = step(of, do_hi, do_lo)
    vcopy[...] = (decode(wv[...], WEIGHT_RATE) - sv[...]).astype(BF16)
    ocopy[...] = (decode(wo[...], WEIGHT_RATE) - so[...]).T.astype(BF16)

    @pl.when(j == fs // 8)
    def _():
        rows = pl.ds(pl.multiple_of(lax.rem(fs, 8) * WIDTH_ROWS, WIDTH_ROWS), WIDTH_ROWS)
        vmaster[...] = vw[...] - sv[rows]
        turn[0:WIDTH_ROWS] = so[rows]
        omaster[...] = ow[...] - turn[...].T[:, :WIDTH_ROWS]


def local(
    inputs, value_cotangent, first_map, second_map, lambdas, head_gain, output_cotangent,
    value_factor, output_factor, value_weight, output_weight,
    value_moment, value_second, output_moment, output_second,
):
    gain = head_gain.reshape(1, HEAD)
    any_spec = pl.BlockSpec(memory_space=pl.ANY)
    dma = pltpu.SemaphoreType.DMA
    vmem = pltpu.VMEM
    sems = [dma((13,)), dma((5,)), dma((2,)), dma((2,)), dma((4,)), dma((4,)), dma((4,)), dma((4,)), dma((4,)), dma((4,))]
    sems += [dma((8,))] * 24
    wv, wo, da, db, low = pl.pallas_call(
        exchange_kernel,
        out_shape=[
            jax.ShapeDtypeStruct((Z, Y, WIDTH_ROWS, 256), BF16),
            jax.ShapeDtypeStruct((Z, Y, WIDTH_ROWS, 256), BF16),
            jax.ShapeDtypeStruct((Z, Y, 8, 128), BF16),
            jax.ShapeDtypeStruct((Y, Z, 8, 128), BF16),
            jax.ShapeDtypeStruct((8, 256), F32),
        ],
        in_specs=[any_spec] * 5
        + [pl.BlockSpec(memory_space=pltpu.SMEM), pl.BlockSpec(memory_space=pltpu.VMEM)]
        + [any_spec] * 8,
        out_specs=[any_spec] * 5,
        scratch_shapes=[
            vmem((512, 256), BF16), vmem((512, 256), BF16), vmem((512, 256), BF16),
            vmem((512, 256), BF16), vmem((512, 256), BF16),
            vmem((512, 256), BF16), vmem((512, 256), BF16),
            vmem((WIDTH_ROWS, 256), F32), vmem((256, WIDTH_ROWS), F32),
            vmem((8, 256), F32), vmem((8, 256), F32),
            vmem((2, 256, 256), BF16), vmem((X, 64, 512), F32), vmem((X, 64, 512), BF16),
            vmem((X, 64, 512), BF16), vmem((C, X, 64, 512), BF16), vmem((512, 256), BF16),
            vmem((Z, Y, 8, 128), BF16), vmem((Y, Z, 8, 128), BF16),
            vmem((Z, Y, 8, 128), BF16), vmem((Y, Z, 8, 128), BF16),
            vmem((Y, 8, 128), F32), vmem((Z, 8, 128), F32),
            vmem((Y, 8, 128), F32), vmem((Z, 8, 128), F32),
            vmem((Z, Y, 8, 128), BF16), vmem((Y, Z, 8, 128), BF16),
            vmem((Z, Y, WIDTH_ROWS, 256), BF16), vmem((Z, Y, WIDTH_ROWS, 256), BF16),
            vmem((8, 256), F32),
        ]
        + sems,
        compiler_params=pltpu.CompilerParams(
            collective_id=0, has_side_effects=True, vmem_limit_bytes=24 * 1024 * 1024
        ),
        name="exchange",
    )(
        inputs, output_cotangent, value_cotangent, first_map, second_map, lambdas, gain,
        value_factor, output_factor, value_weight, output_weight,
        value_moment, value_second, output_moment, output_second,
    )
    width, cols = 2048, 256
    wv, wo = wv.reshape(width, cols), wo.reshape(width, cols)

    def whole(shape):
        return pl.BlockSpec(shape, lambda j: (0,) * len(shape))

    rows = pl.BlockSpec((256, cols), lambda j: (j, 0))
    return pl.pallas_call(
        finish_kernel,
        grid=(width // 256,),
        out_shape=[
            jax.ShapeDtypeStruct((WIDTH_ROWS, cols), F32),
            jax.ShapeDtypeStruct((cols, WIDTH_ROWS), F32),
            jax.ShapeDtypeStruct((4, cols), F32),
            jax.ShapeDtypeStruct((4, cols), F32),
            jax.ShapeDtypeStruct((4, cols), F32),
            jax.ShapeDtypeStruct((4, cols), F32),
            jax.ShapeDtypeStruct((width, cols), BF16),
            jax.ShapeDtypeStruct((cols, width), BF16),
        ],
        in_specs=[
            whole((Z, Y, 8, 128)), whole((Y, Z, 8, 128)), rows, rows, rows, rows,
            whole((8, cols)), whole((WIDTH_ROWS, cols)), whole((cols, WIDTH_ROWS)),
            whole((4, cols)), whole((4, cols)), whole((4, cols)), whole((4, cols)),
        ],
        out_specs=[
            whole((WIDTH_ROWS, cols)), whole((cols, WIDTH_ROWS)),
            whole((4, cols)), whole((4, cols)), whole((4, cols)), whole((4, cols)),
            rows, pl.BlockSpec((cols, 256), lambda j: (0, j)),
        ],
        scratch_shapes=[vmem((RANK, cols), BF16)] * 4
        + [vmem((256, cols), F32)] * 2
        + [vmem((128, cols), F32)],
        name="finish",
    )(
        da, db, wv, wo, value_factor, output_factor, low, value_weight, output_weight,
        value_moment, value_second, output_moment, output_second,
    )


def solution(mesh):
    both = P("fs", "tp")
    in_specs = (
        both, both, both, both, P("tp"), P(), both, P(), P(), both, P("tp", "fs"),
        both, both, both, both,
    )
    out_specs = (
        both, P("tp", "fs"), both, both, both, both, P(None, "tp"), P("tp", None),
    )
    return jax.shard_map(local, mesh=mesh, in_specs=in_specs, out_specs=out_specs, check_vma=False)
```

time: 207 us -> 76.6 us (0.37)
  the two profiles are of different devices: /device:TPU:6 before, /device:TPU:1 now
where the time goes in v1:
time: 76.6 us; the launch traced here: 76 us
  Pallas kernels  61.7 us (81%)
  local copies, waits for them, and re-layouts  13.6 us (18%)
  between operations  0.79 us (1%)
    pallas_call x1, Pallas kernels, local(): pl.pallas_call(exchange_kernel, out_shape=[jax.ShapeDtypeStruct((Z, Y, WI...  53.2 us
    unnamed x41, local copies, waits for them, and re-layouts  12 us
    pallas_call x1, Pallas kernels, local(): pl.pallas_call(finish_kernel, grid=(width // 256,), out_shape=[jax.ShapeD...  8.45 us
    pallas_call x1, local copies, waits for them, and re-layouts, local(): pl.pallas_call(finish_kernel, grid=(width // 256,), out_shape=[jax.ShapeD...  1.59 us

profile of v1, /device:TPU:1, one launch (start us, length us, event | category | flops | bytes accessed | tf_op | source)
XLA Modules:
  0.0 76.0 jit_solution(6965657695136244109)
XLA Ops:
  0.6 0.0 copy-start.10
  0.6 0.0 copy-start.13
  0.7 0.0 copy-start.14
  0.7 0.0 copy-start.15
  0.7 0.0 copy-start.16
  0.7 0.9 %copy.23.ow = f32[256,32]{1,0:T(8,128)S(1)} copy(f32[256,32]{0,1:T(8,128)} %param.25) | data formatting | bytes 65536 | tf_op args[10]
  1.6 0.0 copy-done.10
  1.6 0.0 copy-done.13
  1.7 0.0 copy-start
  1.7 1.2 %copy-done = bf16[2048,256]{1,0:T(8,128)(2,1)S(1)} copy-done((bf16[2048,256]{1,0:T(8,128)(2,1)S(1)}, bf16[2048,256]{1,0:T(8,128)(2,1)}, u32[]{:S(2)}) %copy-start) | copy-done | bytes 1048600
  2.9 1.2 %copy-done.1 = bf16[2048,256]{1,0:T(8,128)(2,1)S(1)} copy-done((bf16[2048,256]{1,0:T(8,128)(2,1)S(1)}, bf16[2048,256]{1,0:T(8,128)(2,1)}, u32[]{:S(2)}) %copy-start.1) | copy-done | bytes 1048600
  4.1 0.9 %copy-done.5 = bf16[512,256]{1,0:T(8,128)(2,1)S(1)} copy-done((bf16[512,256]{1,0:T(8,128)(2,1)S(1)}, bf16[512,256]{1,0:T(8,128)(2,1)}, u32[]{:S(2)}) %copy-start.5) | copy-done | bytes 262168
  5.1 0.9 %copy-done.6 = bf16[512,256]{1,0:T(8,128)(2,1)S(1)} copy-done((bf16[512,256]{1,0:T(8,128)(2,1)S(1)}, bf16[512,256]{1,0:T(8,128)(2,1)}, u32[]{:S(2)}) %copy-start.6) | copy-done | bytes 262168
  6.0 0.9 %copy-done.7 = bf16[512,256]{1,0:T(8,128)(2,1)S(1)} copy-done((bf16[512,256]{1,0:T(8,128)(2,1)S(1)}, bf16[512,256]{1,0:T(8,128)(2,1)}, u32[]{:S(2)}) %copy-start.7) | copy-done | bytes 262168
  7.0 0.9 %copy-done.8 = bf16[512,256]{1,0:T(8,128)(2,1)S(1)} copy-done((bf16[512,256]{1,0:T(8,128)(2,1)S(1)}, bf16[512,256]{1,0:T(8,128)(2,1)}, u32[]{:S(2)}) %copy-start.8) | copy-done | bytes 262168
  7.9 0.9 %copy-done.9 = bf16[512,256]{1,0:T(8,128)(2,1)S(1)} copy-done((bf16[512,256]{1,0:T(8,128)(2,1)S(1)}, bf16[512,256]{1,0:T(8,128)(2,1)}, u32[]{:S(2)}) %copy-start.9) | copy-done | bytes 262168
  8.9 53.2 %exchange.1 = (bf16[8,8,32,256]{3,2,1,0:T(8,128)(2,1)S(1)}, bf16[8,8,32,256]{3,2,1,0:T(8,128)(2,1)S(1)}, bf16[8,8,8,128]{3,2,1,0:T(8,128)(2,1)S(1)}, bf16[8,8,8,128]{3,2,1,0:T(8,128)(2,1)S(1)}, f32[8,256]{1,0:T(8,128)S(1)}) custom-call(bf16[512,256]{1,0:T(8,128)(2,1)S(1)} %copy-done.5, bf16[512,256]{1,0:T(8,128)(2,1)S(1)} %copy-done.6, ...), custom_call_target="tpu_custom_call" | custom-call | tf_op jit(solution)/shard_map/exchange/pallas_call | solution.py:358
  62.1 1.0 %copy-done.3 = bf16[8,8,32,256]{3,2,1,0:T(8,128)(2,1)} copy-done((bf16[8,8,32,256]{3,2,1,0:T(8,128)(2,1)}, bf16[8,8,32,256]{3,2,1,0:T(8,128)(2,1)S(1)}, u32[]{:S(2)}) %copy-start.3) | copy-done | bytes 1048600
  63.1 1.0 %copy-done.4 = bf16[8,8,32,256]{3,2,1,0:T(8,128)(2,1)} copy-done((bf16[8,8,32,256]{3,2,1,0:T(8,128)(2,1)}, bf16[8,8,32,256]{3,2,1,0:T(8,128)(2,1)S(1)}, u32[]{:S(2)}) %copy-start.4) | copy-done | bytes 1048600
  64.1 0.6 copy-done.11
  64.7 0.6 copy-done.12
  65.4 0.6 copy-done.17
  66.0 8.5 %finish.1 = (f32[32,256]{1,0:T(8,128)}, f32[256,32]{1,0:T(8,128)}, f32[4,256]{1,0:T(4,128)}, f32[4,256]{1,0:T(4,128)}, f32[4,256]{1,0:T(4,128)}, /*index=5*/f32[...) custom-call(bf16[8,8,8,128]{3,2,1,0:T(8,128)(2,1)} %copy-done.11, bf16[8,8,8,128]{3,2,1,0:T(8,128)(2,1)} %copy-done.12, ...), custom_call_target="tpu_custom_call" | custom-call | tf_op jit(solution)/shard_map/finish/pallas_call | solution.py:404
  74.4 1.6 %copy.25 = f32[256,32]{0,1:T(8,128)} copy(f32[256,32]{1,0:T(8,128)} %get-tuple-element.19) | data formatting | bytes 65536 | tf_op jit(solution)/shard_map/finish/pallas_call | solution.py:404
  (20 shorter events, 0.0 us)
Async XLA Ops:
  0.6 1.0 %copy-start.10 = (f32[32,256]{1,0:T(8,128)S(1)}, f32[32,256]{1,0:T(8,128)}, u32[]{:S(2)}) copy-start(f32[32,256]{1,0:T(8,128)} %vw.3) | copy-start | bytes 98308
  0.6 1.0 %copy-start.13 = (f32[4,256]{1,0:T(4,128)S(1)}, f32[4,256]{1,0:T(4,128)}, u32[]{:S(2)}) copy-start(f32[4,256]{1,0:T(4,128)} %vm.3) | copy-start | bytes 12292
  0.7 1.0 %copy-start.14 = (f32[4,256]{1,0:T(4,128)S(1)}, f32[4,256]{1,0:T(4,128)}, u32[]{:S(2)}) copy-start(f32[4,256]{1,0:T(4,128)} %vs.3) | copy-start | bytes 12292
  0.7 1.0 %copy-start.15 = (f32[4,256]{1,0:T(4,128)S(1)}, f32[4,256]{1,0:T(4,128)}, u32[]{:S(2)}) copy-start(f32[4,256]{1,0:T(4,128)} %om.3) | copy-start | bytes 12292
  0.7 1.0 %copy-start.16 = (f32[4,256]{1,0:T(4,128)S(1)}, f32[4,256]{1,0:T(4,128)}, u32[]{:S(2)}) copy-start(f32[4,256]{1,0:T(4,128)} %os_.3) | copy-start | bytes 12292
  0.7 1.0 %copy-start.18 = (f32[2]{0:T(128)S(1)}, f32[2]{0:T(128)}, u32[]{:S(2)}) copy-start(f32[2]{0:T(128)} %lambdas.1) | copy-start | bytes 28
  0.7 1.0 %copy-start.19 = (f32[128]{0:T(128)S(1)}, f32[128]{0:T(128)}, u32[]{:S(2)}) copy-start(f32[128]{0:T(128)} %param.20) | copy-start | bytes 1540
  1.7 1.2 %copy-start = (bf16[2048,256]{1,0:T(8,128)(2,1)S(1)}, bf16[2048,256]{1,0:T(8,128)(2,1)}, u32[]{:S(2)}) copy-start(bf16[2048,256]{1,0:T(8,128)(2,1)} %vf.3) | copy-start | bytes 3145732
  2.9 1.2 %copy-start.1 = (bf16[2048,256]{1,0:T(8,128)(2,1)S(1)}, bf16[2048,256]{1,0:T(8,128)(2,1)}, u32[]{:S(2)}) copy-start(bf16[2048,256]{1,0:T(8,128)(2,1)} %of.3) | copy-start | bytes 3145732
  4.1 0.9 %copy-start.5 = (bf16[512,256]{1,0:T(8,128)(2,1)S(1)}, bf16[512,256]{1,0:T(8,128)(2,1)}, u32[]{:S(2)}) copy-start(bf16[512,256]{1,0:T(8,128)(2,1)} %inputs.1) | copy-start | bytes 786436
  5.1 0.9 %copy-start.6 = (bf16[512,256]{1,0:T(8,128)(2,1)S(1)}, bf16[512,256]{1,0:T(8,128)(2,1)}, u32[]{:S(2)}) copy-start(bf16[512,256]{1,0:T(8,128)(2,1)} %ocot.1) | copy-start | bytes 786436
  6.0 0.9 %copy-start.7 = (bf16[512,256]{1,0:T(8,128)(2,1)S(1)}, bf16[512,256]{1,0:T(8,128)(2,1)}, u32[]{:S(2)}) copy-start(bf16[512,256]{1,0:T(8,128)(2,1)} %vcot.1) | copy-start | bytes 786436
  7.0 0.9 %copy-start.8 = (bf16[512,256]{1,0:T(8,128)(2,1)S(1)}, bf16[512,256]{1,0:T(8,128)(2,1)}, u32[]{:S(2)}) copy-start(bf16[512,256]{1,0:T(8,128)(2,1)} %first.1) | copy-start | bytes 786436
  7.9 0.9 %copy-start.9 = (bf16[512,256]{1,0:T(8,128)(2,1)S(1)}, bf16[512,256]{1,0:T(8,128)(2,1)}, u32[]{:S(2)}) copy-start(bf16[512,256]{1,0:T(8,128)(2,1)} %second.1) | copy-start | bytes 786436
  8.9 53.2 %copy-start.2 = (f32[256,32]{1,0:T(8,128)}, f32[256,32]{1,0:T(8,128)S(1)}, u32[]{:S(2)}) copy-start(f32[256,32]{1,0:T(8,128)S(1)} %copy.23.ow) | copy-start | bytes 98308
  62.1 1.0 %copy-start.3 = (bf16[8,8,32,256]{3,2,1,0:T(8,128)(2,1)}, bf16[8,8,32,256]{3,2,1,0:T(8,128)(2,1)S(1)}, u32[]{:S(2)}) copy-start(bf16[8,8,32,256]{3,2,1,0:T(8,128)(2,1)S(1)} %get-tuple-element.15) | copy-start | bytes 3145732
  63.1 1.0 %copy-start.4 = (bf16[8,8,32,256]{3,2,1,0:T(8,128)(2,1)}, bf16[8,8,32,256]{3,2,1,0:T(8,128)(2,1)S(1)}, u32[]{:S(2)}) copy-start(bf16[8,8,32,256]{3,2,1,0:T(8,128)(2,1)S(1)} %get-tuple-element.16) | copy-start | bytes 3145732
  64.1 0.6 copy-start.11
  64.7 0.6 copy-start.12
  65.4 0.6 copy-start.17

commit v2 on v1

v2 whole, which is shorter than its diff:
```python
import functools
import math

import jax
import jax.numpy as jnp
from jax import lax
from jax.experimental import pallas as pl
from jax.experimental.pallas import tpu as pltpu
from jax.sharding import PartitionSpec as P

MESH = pl.DeviceIdType.MESH
X, C, Y, Z = 4, 2, 8, 8
F32, BF16 = jnp.float32, jnp.bfloat16
RANK, HEAD = 256, 128
FAR = (4, 3, 5, 2, 6, 1, 7)
NEAR = (1, 7, 2, 6, 3, 5, 4)
WIDTH_ROWS = 32
STEP = 512
WEIGHT_RATE = 960.0
DIRECTION_RATE = 11.0


def encode(value, rate):
    size = jnp.exp2(jnp.abs(value) * rate) - 1.0
    return jnp.where(value < 0, -size, size).astype(BF16)


def decode(code, rate):
    code = code.astype(F32)
    size = jnp.log(1.0 + jnp.abs(code)) * (1.0 / (rate * math.log(2.0)))
    return jnp.where(code < 0, -size, size)


def rows_dot(left, right):
    return lax.dot_general(left, right, (((0,), (0,)), ((), ())), preferred_element_type=F32)


def exchange_kernel(
    inputs, ocot, vcot, first, second, lambdas, gain, vf, of, vw, ow, vm, vs, om, os_,
    wv_out, wo_out, da_out, db_out, low_out,
    in_v, oc_v, vc_v, fi_v, se_v, vf_v, of_v, vw_v, ow_v, mom_v, sec_v,
    pair, ax, sx, rx, pq, heads,
    la, lb, ra, rb, sa, sb, ra2, rb2, da, db, wv, wo, low_v, wv_f, wo_f,
    load_sem, out_sem,
    pair_s, pair_r, xs_s, xs_r, xg_s, xg_r, fw_s, fw_r,
    r1a_s, r1a_r, r1b_s, r1b_r, r2a_s, r2a_r, r2b_s, r2b_r,
    g1a_s, g1a_r, g1b_s, g1b_r, g2a_s, g2a_r, g2b_s, g2b_r,
    w1v_s, w1v_r, w1o_s, w1o_r, wrv_s, wrv_r, wro_s, wro_r,
):
    fs = lax.axis_index("fs")
    tp = lax.axis_index("tp")
    z, y = fs // Y, lax.rem(fs, Y)
    x, c = tp // C, lax.rem(tp, C)

    def at_x(d):
        return (fs, lax.rem(x + d, X) * C + c)

    def at_y(d):
        return (z * Y + lax.rem(y + d, Y), tp)

    def at_z(d):
        return (lax.rem(z + d, Z) * Y + y, tp)

    partner = (fs, x * C + (1 - c))

    def send(src, dst, s, r, where):
        copy = pltpu.make_async_remote_copy(
            src_ref=src, dst_ref=dst, send_sem=s, recv_sem=r, device_id=where, device_id_type=MESH
        )
        copy.start()
        return copy

    chip_rows = pl.ds(pl.multiple_of(x * (C * 256), C * 256), C * 256)
    loads = {}
    for i, (name, src, dst) in enumerate(
        [
            ("vw", vw, vw_v),
            ("ow", ow, ow_v),
            ("in", inputs, in_v),
            ("oc", ocot, oc_v),
            ("vf", vf.at[chip_rows], vf_v),
            ("of", of.at[chip_rows], of_v),
            ("fi", first, fi_v),
            ("se", second, se_v),
            ("vc", vcot, vc_v),
            ("vm", vm, mom_v.at[pl.ds(0, 4)]),
            ("om", om, mom_v.at[pl.ds(4, 4)]),
            ("vs", vs, sec_v.at[pl.ds(0, 4)]),
            ("os", os_, sec_v.at[pl.ds(4, 4)]),
        ]
    ):
        loads[name] = pltpu.make_async_copy(src, dst, load_sem.at[i])
        loads[name].start()

    barrier = pltpu.get_barrier_semaphore()
    friends = (
        [partner]
        + [at_x(d) for d in range(1, X)]
        + [at_y(d) for d in range(1, Y)]
        + [at_z(d) for d in range(1, Z)]
    )
    for friend in friends:
        pl.semaphore_signal(barrier, inc=1, device_id=friend, device_id_type=MESH)

    loads["vw"].wait()
    wv[z, y] = encode(vw_v[...], WEIGHT_RATE)
    loads["ow"].wait()
    wo[z, y] = encode(ow_v[...], WEIGHT_RATE)
    loads["in"].wait()
    loads["oc"].wait()
    loads["vf"].wait()
    loads["of"].wait()
    pl.semaphore_wait(barrier, len(friends))

    mine = pl.ds(pl.multiple_of(c * 256, 256), 256)
    theirs = pl.ds(pl.multiple_of((1 - c) * 256, 256), 256)
    to_pair = [
        send(in_v.at[theirs], pair.at[0], pair_s.at[0], pair_r.at[0], partner),
        send(oc_v.at[theirs], pair.at[1], pair_s.at[1], pair_r.at[1], partner),
    ]
    w1v = {
        d: send(wv.at[z, y], wv.at[z, y], w1v_s.at[d], w1v_r.at[d], at_y(d)) for d in FAR
    }
    w1o = {
        d: send(wo.at[z, y], wo.at[z, y], w1o_s.at[d], w1o_r.at[d], at_z(d)) for d in FAR
    }
    acc_p = jnp.dot(in_v[mine], vf_v[mine], preferred_element_type=F32)
    acc_q = jnp.dot(oc_v[mine], of_v[mine], preferred_element_type=F32)
    for copy in to_pair:
        copy.wait_recv()
    acc_p += jnp.dot(pair[0], vf_v[theirs], preferred_element_type=F32)
    acc_q += jnp.dot(pair[1], of_v[theirs], preferred_element_type=F32)
    acc = jnp.concatenate([acc_p, acc_q], axis=1).reshape(X, 64, 512)
    ax[...] = acc
    sx[...] = acc.astype(BF16)
    x_sum = {
        d: send(sx.at[lax.rem(x + d, X)], rx.at[x], xs_s.at[d], xs_r.at[d], at_x(d))
        for d in (2, 1, 3)
    }

    def ring_step(s):
        zr, yr = lax.rem(z + Z - (s - 1), Z), lax.rem(y + Y - (s - 1), Y)
        zl, yl = lax.rem(z + (s - 1), Z), lax.rem(y + (s - 1), Y)
        first_half = pl.ds(0, 8 if s < 4 else 4)
        other_half = pl.ds(0, 8) if s < 4 else pl.ds(4, 4)
        moves = [
            (wv.at[zr, first_half], wrv_s, wrv_r, s, at_z(1)),
            (wo.at[first_half, pl.ds(yr, 1)], wro_s, wro_r, s, at_y(1)),
            (wv.at[zl, other_half], wrv_s, wrv_r, 4 + s, at_z(Z - 1)),
            (wo.at[other_half, pl.ds(yl, 1)], wro_s, wro_r, 4 + s, at_y(Y - 1)),
        ]
        return [send(ref, ref, ss.at[k], rs.at[k], where) for ref, ss, rs, k, where in moves]

    def open_group(at):
        wv_f[at] = decode(wv[at].reshape(256, 256), WEIGHT_RATE)

    for d in NEAR:
        w1v[d].wait_recv()
        w1o[d].wait_recv()
    rings = [ring_step(1)]

    loads["fi"].wait()
    loads["se"].wait()
    for h in range(2):
        cols = slice(h * HEAD, (h + 1) * HEAD)
        difference = fi_v[:, cols].astype(F32) - lambdas[h] * se_v[:, cols].astype(F32)
        mean = jnp.mean(difference * difference, axis=-1, keepdims=True)
        heads[:, cols] = (difference * lax.rsqrt(mean + 1e-06) * gain[...]).astype(BF16)

    total = ax[x]
    for d in (1, 3, 2):
        x_sum[d].wait_recv()
        total += rx[lax.rem(x + X - d, X)].astype(F32)
    pq[c, x] = total.astype(BF16)
    x_all = {
        d: send(pq.at[c, x], pq.at[c, x], xg_s.at[d], xg_r.at[d], at_x(d)) for d in (2, 1, 3)
    }
    passed = [send(pq.at[c, x], pq.at[c, x], fw_s.at[0], fw_r.at[0], partner)]

    for copy in rings[0]:
        copy.wait_recv()
    rings.append(ring_step(2))
    open_group(z)
    open_group(lax.rem(z + Z - 1, Z))
    open_group(lax.rem(z + 1, Z))

    for d in (1, 3, 2):
        x_all[d].wait_recv()
        xx = lax.rem(x + X - d, X)
        passed.append(send(pq.at[c, xx], pq.at[c, xx], fw_s.at[d], fw_r.at[d], partner))
    loads["vc"].wait()
    pq_mine = pq[c].reshape(256, 512)
    lv = rows_dot(pq_mine[:, :RANK], vc_v[mine])
    lo = rows_dot(pq_mine[:, RANK:], heads[mine])
    for copy in rings[1]:
        copy.wait_recv()
    rings.append(ring_step(3))
    for copy in passed:
        copy.wait_recv()
    pq_theirs = pq[1 - c].reshape(256, 512)
    lv += rows_dot(pq_theirs[:, :RANK], vc_v[theirs])
    lo += rows_dot(pq_theirs[:, RANK:], heads[theirs])
    scale = 1.0 / math.sqrt(32768.0)
    lv3 = (lv * scale).reshape(32, 8, 256)
    lo3 = (lo * scale).reshape(32, 8, 256)
    upper = lax.broadcasted_iota(jnp.int32, (32, 8, 256), 1) < 4
    even = jnp.where(upper, lv3, pltpu.roll(lo3, 4, 1)).astype(BF16)
    odd = jnp.where(upper, pltpu.roll(lv3, 4, 1), lo3).astype(BF16)
    for f in range(Z * Y):
        block = (odd if f % 2 else even)[f // 2]
        la[f // Y, f % Y] = block[:, :128]
        lb[f % Y, f // Y] = block[:, 128:]
    r1a, r1b = {}, {}
    for d in FAR:
        r1a[d] = send(la.at[lax.rem(z + d, Z)], ra.at[z], r1a_s.at[d], r1a_r.at[d], at_z(d))
        r1b[d] = send(lb.at[lax.rem(y + d, Y)], rb.at[y], r1b_s.at[d], r1b_r.at[d], at_y(d))

    open_group(lax.rem(z + Z - 2, Z))
    open_group(lax.rem(z + 2, Z))
    for copy in rings[2]:
        copy.wait_recv()
    rings.append(ring_step(4))
    open_group(lax.rem(z + Z - 3, Z))
    open_group(lax.rem(z + 3, Z))

    sum_a = la[z].astype(F32)
    sum_b = lb[y].astype(F32)
    for d in NEAR:
        r1a[d].wait_recv()
        sum_a += ra[lax.rem(z + Z - d, Z)].astype(F32)
        r1b[d].wait_recv()
        sum_b += rb[lax.rem(y + Y - d, Y)].astype(F32)
    sa[...] = sum_a
    sb[...] = sum_b
    r2a, r2b = {}, {}
    for d in FAR:
        r2a[d] = send(sa.at[lax.rem(y + d, Y)], ra2.at[y], r2a_s.at[d], r2a_r.at[d], at_y(d))
        r2b[d] = send(sb.at[lax.rem(z + d, Z)], rb2.at[z], r2b_s.at[d], r2b_r.at[d], at_z(d))

    for copy in rings[3]:
        copy.wait_recv()
    open_group(lax.rem(z + 4, Z))
    for k in range(Z // 2):
        wo_f[:, k * 256 : (k + 1) * 256] = decode(wo[k].reshape(256, 256).T, WEIGHT_RATE)

    low_a = sa[y]
    low_b = sb[z]
    for d in NEAR:
        r2a[d].wait_recv()
        low_a += ra2[lax.rem(y + Y - d, Y)]
        r2b[d].wait_recv()
        low_b += rb2[lax.rem(z + Z - d, Z)]
    low = jnp.concatenate([low_a, low_b], axis=1)
    low_v[...] = low
    for name in ("vm", "om", "vs", "os"):
        loads[name].wait()
    moment = 0.8 * mom_v[...] + 0.2 * low
    spread = 0.95 * sec_v[...] + 0.05 * low * low
    code = encode(moment / (jnp.sqrt(spread) + 1e-08), DIRECTION_RATE)
    da[z, y] = code[:, :128]
    db[y, z] = code[:, 128:]
    g1a, g1b, g2a, g2b = {}, {}, {}, {}
    for d in FAR:
        g1a[d] = send(da.at[z, y], da.at[z, y], g1a_s.at[d], g1a_r.at[d], at_y(d))
        g1b[d] = send(db.at[y, z], db.at[y, z], g1b_s.at[d], g1b_r.at[d], at_z(d))

    for k in range(Z // 2, Z):
        wo_f[:, k * 256 : (k + 1) * 256] = decode(wo[k].reshape(256, 256).T, WEIGHT_RATE)
    outs = [
        pltpu.make_async_copy(wv_f, wv_out, out_sem.at[0]),
        pltpu.make_async_copy(wo_f, wo_out, out_sem.at[1]),
        pltpu.make_async_copy(low_v, low_out, out_sem.at[2]),
    ]
    for copy in outs:
        copy.start()

    for d in NEAR:
        g1a[d].wait_recv()
    for d in FAR:
        g2a[d] = send(da.at[z], da.at[z], g2a_s.at[d], g2a_r.at[d], at_z(d))
    for d in NEAR:
        g1b[d].wait_recv()
    for d in FAR:
        g2b[d] = send(db.at[y], db.at[y], g2b_s.at[d], g2b_r.at[d], at_y(d))
    for d in NEAR:
        g2a[d].wait_recv()
        g2b[d].wait_recv()
    last = [
        pltpu.make_async_copy(da, da_out, out_sem.at[3]),
        pltpu.make_async_copy(db, db_out, out_sem.at[4]),
    ]
    for copy in last:
        copy.start()
    sent = to_pair + passed
    for group in (w1v, w1o, x_sum, x_all, r1a, r1b, r2a, r2b, g1a, g1b, g2a, g2b):
        sent += list(group.values())
    for ring in rings:
        sent += ring
    for copy in sent:
        copy.wait_send()
    for copy in outs + last:
        copy.wait()


def finish_kernel(
    da, db, wv, wo, vf, of, low, vw, ow, vm, vs, om, os_,
    vmaster, omaster, vm_new, vs_new, om_new, os_new, vcopy, ocopy,
    dv, do, do_t,
):
    j = pl.program_id(0)
    fs = lax.axis_index("fs")

    @pl.when(j == 0)
    def _():
        low_v, low_o = low[0:4], low[4:8]
        vm_new[...] = 0.8 * vm[...] + 0.2 * low_v
        vs_new[...] = 0.95 * vs[...] + 0.05 * low_v * low_v
        om_new[...] = 0.8 * om[...] + 0.2 * low_o
        os_new[...] = 0.95 * os_[...] + 0.05 * low_o * low_o
        upper = lax.broadcasted_iota(jnp.int32, (8, 256), 0) < 4
        for g in range(Z * Y // 2):
            zz, yy = (2 * g) // Y, (2 * g) % Y
            even = jnp.concatenate([da[zz, yy], db[yy, zz]], axis=1)
            odd = jnp.concatenate([da[zz, yy + 1], db[yy + 1, zz]], axis=1)
            even = 0.05 * decode(even, DIRECTION_RATE)
            odd = 0.05 * decode(odd, DIRECTION_RATE)
            value = jnp.where(upper, even, pltpu.roll(odd, 4, 0))
            output = jnp.where(upper, pltpu.roll(even, 4, 0), odd)
            for full, both in ((value, dv), (output, do)):
                top = full.astype(BF16)
                both[8 * g : 8 * g + 8] = top
                both[RANK + 8 * g : RANK + 8 * g + 8] = (full - top.astype(F32)).astype(BF16)
        do_t[...] = do[...].T

    factor_v = vf[...]
    step_v = jnp.dot(
        jnp.concatenate([factor_v, factor_v], axis=1), dv[...], preferred_element_type=F32
    )
    vcopy[...] = (wv[...] - step_v).astype(BF16)
    factor_o = of[...]
    step_o = lax.dot_general(
        do_t[...],
        jnp.concatenate([factor_o, factor_o], axis=1),
        (((1,), (1,)), ((), ())),
        preferred_element_type=F32,
    )
    ocopy[...] = (wo[...] - step_o).astype(BF16)

    @pl.when(j == fs // (STEP // WIDTH_ROWS))
    def _():
        at = lax.rem(fs, STEP // WIDTH_ROWS) * WIDTH_ROWS
        rows = pl.ds(pl.multiple_of(at, WIDTH_ROWS), WIDTH_ROWS)
        for factor, both, weight, out in ((vf, dv, vw, vmaster), (of, do, ow, omaster)):
            own = factor[rows]
            out[...] = weight[...] - jnp.dot(
                jnp.concatenate([own, own], axis=1), both[...], preferred_element_type=F32
            )


def local(
    inputs, value_cotangent, first_map, second_map, lambdas, head_gain, output_cotangent,
    value_factor, output_factor, value_weight, output_weight,
    value_moment, value_second, output_moment, output_second,
):
    turned_weight = output_weight.T
    gain = head_gain.reshape(1, HEAD)
    any_spec = pl.BlockSpec(memory_space=pl.ANY)
    dma = pltpu.SemaphoreType.DMA
    vmem = pltpu.VMEM
    sems = [dma((13,)), dma((5,)), dma((2,)), dma((2,)), dma((4,)), dma((4,)), dma((4,)), dma((4,)), dma((4,)), dma((4,))]
    sems += [dma((8,))] * 20 + [dma((9,))] * 4
    wv, wo, da, db, low = pl.pallas_call(
        exchange_kernel,
        out_shape=[
            jax.ShapeDtypeStruct((Z, 256, 256), F32),
            jax.ShapeDtypeStruct((256, 2048), F32),
            jax.ShapeDtypeStruct((Z, Y, 8, 128), BF16),
            jax.ShapeDtypeStruct((Y, Z, 8, 128), BF16),
            jax.ShapeDtypeStruct((8, 256), F32),
        ],
        in_specs=[any_spec] * 5
        + [pl.BlockSpec(memory_space=pltpu.SMEM), pl.BlockSpec(memory_space=pltpu.VMEM)]
        + [any_spec] * 8,
        out_specs=[any_spec] * 5,
        scratch_shapes=[
            vmem((512, 256), BF16), vmem((512, 256), BF16), vmem((512, 256), BF16),
            vmem((512, 256), BF16), vmem((512, 256), BF16),
            vmem((512, 256), BF16), vmem((512, 256), BF16),
            vmem((WIDTH_ROWS, 256), F32), vmem((WIDTH_ROWS, 256), F32),
            vmem((8, 256), F32), vmem((8, 256), F32),
            vmem((2, 256, 256), BF16), vmem((X, 64, 512), F32), vmem((X, 64, 512), BF16),
            vmem((X, 64, 512), BF16), vmem((C, X, 64, 512), BF16), vmem((512, 256), BF16),
            vmem((Z, Y, 8, 128), BF16), vmem((Y, Z, 8, 128), BF16),
            vmem((Z, Y, 8, 128), BF16), vmem((Y, Z, 8, 128), BF16),
            vmem((Y, 8, 128), F32), vmem((Z, 8, 128), F32),
            vmem((Y, 8, 128), F32), vmem((Z, 8, 128), F32),
            vmem((Z, Y, 8, 128), BF16), vmem((Y, Z, 8, 128), BF16),
            vmem((Z, Y, WIDTH_ROWS, 256), BF16), vmem((Z, Y, WIDTH_ROWS, 256), BF16),
            vmem((8, 256), F32), vmem((Z, 256, 256), F32), vmem((256, 2048), F32),
        ]
        + sems,
        compiler_params=pltpu.CompilerParams(
            collective_id=0, has_side_effects=True, vmem_limit_bytes=60 * 1024 * 1024
        ),
        name="exchange",
    )(
        inputs, output_cotangent, value_cotangent, first_map, second_map, lambdas, gain,
        value_factor, output_factor, value_weight, turned_weight,
        value_moment, value_second, output_moment, output_second,
    )
    width, cols = 2048, 256
    wv = wv.reshape(width, cols)

    def whole(shape):
        return pl.BlockSpec(shape, lambda j: (0,) * len(shape))

    rows = pl.BlockSpec((STEP, cols), lambda j: (j, 0))
    turned = pl.BlockSpec((cols, STEP), lambda j: (0, j))
    vmaster, omaster, *rest = pl.pallas_call(
        finish_kernel,
        grid=(width // STEP,),
        out_shape=[
            jax.ShapeDtypeStruct((WIDTH_ROWS, cols), F32),
            jax.ShapeDtypeStruct((WIDTH_ROWS, cols), F32),
            jax.ShapeDtypeStruct((4, cols), F32),
            jax.ShapeDtypeStruct((4, cols), F32),
            jax.ShapeDtypeStruct((4, cols), F32),
            jax.ShapeDtypeStruct((4, cols), F32),
            jax.ShapeDtypeStruct((width, cols), BF16),
            jax.ShapeDtypeStruct((cols, width), BF16),
        ],
        in_specs=[
            whole((Z, Y, 8, 128)), whole((Y, Z, 8, 128)), rows, turned, rows, rows,
            whole((8, cols)), whole((WIDTH_ROWS, cols)), whole((WIDTH_ROWS, cols)),
            whole((4, cols)), whole((4, cols)), whole((4, cols)), whole((4, cols)),
        ],
        out_specs=[
            whole((WIDTH_ROWS, cols)), whole((WIDTH_ROWS, cols)),
            whole((4, cols)), whole((4, cols)), whole((4, cols)), whole((4, cols)),
            rows, turned,
        ],
        scratch_shapes=[
            vmem((2 * RANK, cols), BF16), vmem((2 * RANK, cols), BF16), vmem((cols, 2 * RANK), BF16),
        ],
        compiler_params=pltpu.CompilerParams(vmem_limit_bytes=60 * 1024 * 1024),
        name="finish",
    )(
        da, db, wv, wo, value_factor, output_factor, low, value_weight, turned_weight,
        value_moment, value_second, output_moment, output_second,
    )
    return (vmaster, omaster.T, *rest)


def solution(mesh):
    both = P("fs", "tp")
    in_specs = (
        both, both, both, both, P("tp"), P(), both, P(), P(), both, P("tp", "fs"),
        both, both, both, both,
    )
    out_specs = (
        both, P("tp", "fs"), both, both, both, both, P(None, "tp"), P("tp", None),
    )
    return jax.shard_map(local, mesh=mesh, in_specs=in_specs, out_specs=out_specs, check_vma=False)
```

time: 76.6 us -> 62.5 us (0.82)
  the two profiles are of different devices: /device:TPU:1 before, /device:TPU:6 now
where the time goes in v2:
time: 62.5 us; the launch traced here: 62.2 us
  Pallas kernels  61.5 us (98%)
  between operations  0.64 us (1%)
    pallas_call x1, Pallas kernels, local(): pl.pallas_call(exchange_kernel, out_shape=[jax.ShapeDtypeStruct((Z, 256,...  55.2 us
    pallas_call x1, Pallas kernels, local(): pl.pallas_call(finish_kernel, grid=(width // STEP,), out_shape=[jax.Shape...  6.27 us

profile of v2, /device:TPU:6, one launch (start us, length us, event | category | flops | bytes accessed | tf_op | source)
XLA Modules:
  0.0 62.2 jit_solution(8990984820220124601)
XLA Ops:
  0.6 55.2 %exchange.1 = (f32[8,256,256]{2,1,0:T(8,128)}, f32[256,2048]{1,0:T(8,128)}, bf16[8,8,8,128]{3,2,1,0:T(8,128)(2,1)}, bf16[8,8,8,128]{3,2,1,0:T(8,128)(2,1)}, f32[8,256]{1,0:T(8,128)}) custom-call(bf16[512,256]{1,0:T(8,128)(2,1)} %inputs.1, bf16[512,256]{1,0:T(8,128)(2,1)} %ocot.1, bf16[512,256]{1,0:T(8,128)(2,1)} %vcot.1, bf16[512,256]{1,0:T(8,128)(2,1)} %first.1, ...), custom_call_target="tpu_custom_call" | custom-call | tf_op jit(solution)/shard_map/exchange/pallas_call | solution.py:372
  55.9 6.3 %finish.1 = (f32[32,256]{1,0:T(8,128)}, f32[32,256]{1,0:T(8,128)}, f32[4,256]{1,0:T(4,128)}, f32[4,256]{1,0:T(4,128)}, f32[4,256]{1,0:T(4,128)}, /*index=5*/f32[...) custom-call(bf16[8,8,8,128]{3,2,1,0:T(8,128)(2,1)} %get-tuple-element.21.da, ...), custom_call_target="tpu_custom_call" | custom-call | tf_op jit(solution)/shard_map/finish/pallas_call | solution.py:419

commit v3 on v2

v3 whole, which is shorter than its diff:
```python
import functools
import math

import jax
import jax.numpy as jnp
from jax import lax
from jax.experimental import pallas as pl
from jax.experimental.pallas import tpu as pltpu
from jax.sharding import PartitionSpec as P

MESH = pl.DeviceIdType.MESH
X, C, Y, Z = 4, 2, 8, 8
F32, BF16 = jnp.float32, jnp.bfloat16
RANK, HEAD = 256, 128
FAR = (4, 3, 5, 2, 6, 1, 7)
NEAR = (1, 7, 2, 6, 3, 5, 4)
WIDTH_ROWS = 32
STEP = 512
CHUNKS = 2048 // STEP
WEIGHT_RATE = 960.0
DIRECTION_RATE = 11.0


def encode(value, rate):
    size = jnp.exp2(jnp.abs(value) * rate) - 1.0
    return jnp.where(value < 0, -size, size).astype(BF16)


def decode(code, rate):
    code = code.astype(F32)
    size = jnp.log(1.0 + jnp.abs(code)) * (1.0 / (rate * math.log(2.0)))
    return jnp.where(code < 0, -size, size)


def rows_dot(left, right):
    return lax.dot_general(left, right, (((0,), (0,)), ((), ())), preferred_element_type=F32)


def exchange_kernel(
    inputs, ocot, vcot, first, second, lambdas, gain, vf, of, vw, ow, vm, vs, om, os_,
    wv_f, wo_f, da, db, low_v,
    in_v, oc_v, vc_v, fi_v, se_v, vf_v, of_v, vw_v, ow_v, mom_v, sec_v,
    pair, ax, sx, rx, pq, heads,
    la, lb, ra, rb, sa, sb, ra2, rb2, wv, wo,
    load_sem,
    pair_s, pair_r, xs_s, xs_r, xg_s, xg_r, fw_s, fw_r,
    r1a_s, r1a_r, r1b_s, r1b_r, r2a_s, r2a_r, r2b_s, r2b_r,
    g1a_s, g1a_r, g1b_s, g1b_r, g2a_s, g2a_r, g2b_s, g2b_r,
    w1v_s, w1v_r, w1o_s, w1o_r, wrv_s, wrv_r, wro_s, wro_r,
):
    fs = lax.axis_index("fs")
    tp = lax.axis_index("tp")
    z, y = fs // Y, lax.rem(fs, Y)
    x, c = tp // C, lax.rem(tp, C)

    def at_x(d):
        return (fs, lax.rem(x + d, X) * C + c)

    def at_y(d):
        return (z * Y + lax.rem(y + d, Y), tp)

    def at_z(d):
        return (lax.rem(z + d, Z) * Y + y, tp)

    partner = (fs, x * C + (1 - c))

    def send(src, dst, s, r, where):
        copy = pltpu.make_async_remote_copy(
            src_ref=src, dst_ref=dst, send_sem=s, recv_sem=r, device_id=where, device_id_type=MESH
        )
        copy.start()
        return copy

    barrier = pltpu.get_barrier_semaphore()
    friends = (
        [at_y(d) for d in FAR] + [at_z(d) for d in FAR] + [at_x(d) for d in (2, 1, 3)] + [partner]
    )
    for friend in friends:
        pl.semaphore_signal(barrier, inc=1, device_id=friend, device_id_type=MESH)

    chip_rows = pl.ds(pl.multiple_of(x * (C * 256), C * 256), C * 256)
    loads = {}
    for i, (name, src, dst) in enumerate(
        [
            ("vw", vw, vw_v),
            ("ow", ow, ow_v),
            ("in", inputs, in_v),
            ("vf", vf.at[chip_rows], vf_v),
            ("oc", ocot, oc_v),
            ("of", of.at[chip_rows], of_v),
            ("fi", first, fi_v),
            ("se", second, se_v),
            ("vc", vcot, vc_v),
            ("vm", vm, mom_v.at[pl.ds(0, 4)]),
            ("om", om, mom_v.at[pl.ds(4, 4)]),
            ("vs", vs, sec_v.at[pl.ds(0, 4)]),
            ("os", os_, sec_v.at[pl.ds(4, 4)]),
        ]
    ):
        loads[name] = pltpu.make_async_copy(src, dst, load_sem.at[i])
        loads[name].start()

    mine = pl.ds(pl.multiple_of(c * 256, 256), 256)
    theirs = pl.ds(pl.multiple_of((1 - c) * 256, 256), 256)
    pl.semaphore_wait(barrier, len(friends))
    to_pair = [
        send(inputs.at[theirs], pair.at[0], pair_s.at[0], pair_r.at[0], partner),
        send(ocot.at[theirs], pair.at[1], pair_s.at[1], pair_r.at[1], partner),
    ]
    loads["vw"].wait()
    wv[z, y] = encode(vw_v[...], WEIGHT_RATE)
    loads["ow"].wait()
    wo[z, y] = encode(ow_v[...], WEIGHT_RATE)
    w1v, w1o = {}, {}
    for d in FAR:
        w1v[d] = send(wv.at[z, y], wv.at[z, y], w1v_s.at[d], w1v_r.at[d], at_y(d))
        w1o[d] = send(wo.at[z, y], wo.at[z, y], w1o_s.at[d], w1o_r.at[d], at_z(d))
    for name in ("in", "vf", "oc", "of"):
        loads[name].wait()
    acc_p = jnp.dot(in_v[mine], vf_v[mine], preferred_element_type=F32)
    acc_q = jnp.dot(oc_v[mine], of_v[mine], preferred_element_type=F32)
    for copy in to_pair:
        copy.wait_recv()
    acc_p += jnp.dot(pair[0], vf_v[theirs], preferred_element_type=F32)
    acc_q += jnp.dot(pair[1], of_v[theirs], preferred_element_type=F32)
    acc = jnp.concatenate([acc_p, acc_q], axis=1).reshape(X, 64, 512)
    ax[...] = acc
    sx[...] = acc.astype(BF16)
    x_sum = {
        d: send(sx.at[lax.rem(x + d, X)], rx.at[x], xs_s.at[d], xs_r.at[d], at_x(d))
        for d in (2, 1, 3)
    }

    def ring_step(s, h):
        half = pl.ds(h * 4, 4)
        moves = []
        if s < 4 or h == 0:
            zz, yy = lax.rem(z + Z - (s - 1), Z), lax.rem(y + Y - (s - 1), Y)
            k = 4 * (s - 1) + 2 * h
            moves += [(wv.at[zz, half], wrv_s, wrv_r, k, at_z(1))]
            moves += [(wo.at[half, pl.ds(yy, 1)], wro_s, wro_r, k, at_y(1))]
        if s < 4 or h == 1:
            zz, yy = lax.rem(z + (s - 1), Z), lax.rem(y + (s - 1), Y)
            k = 4 * (s - 1) + 2 * h + 1
            moves += [(wv.at[zz, half], wrv_s, wrv_r, k, at_z(Z - 1))]
            moves += [(wo.at[half, pl.ds(yy, 1)], wro_s, wro_r, k, at_y(Y - 1))]
        rings[s, h] = [
            send(ref, ref, ss.at[k], rs.at[k], where) for ref, ss, rs, k, where in moves
        ]

    def ring_wait(s, h):
        for copy in rings[s, h]:
            copy.wait_recv()

    rings = {}

    def open_group(at):
        wv_f[at] = decode(wv[at].reshape(256, 256), WEIGHT_RATE)

    for d in NEAR:
        w1v[d].wait_recv()
        w1o[d].wait_recv()
    ring_step(1, 0)
    ring_step(1, 1)

    loads["fi"].wait()
    loads["se"].wait()
    for h in range(2):
        cols = slice(h * HEAD, (h + 1) * HEAD)
        difference = fi_v[:, cols].astype(F32) - lambdas[h] * se_v[:, cols].astype(F32)
        mean = jnp.mean(difference * difference, axis=-1, keepdims=True)
        heads[:, cols] = (difference * lax.rsqrt(mean + 1e-06) * gain[...]).astype(BF16)

    total = ax[x]
    for d in (1, 3, 2):
        x_sum[d].wait_recv()
        total += rx[lax.rem(x + X - d, X)].astype(F32)
    pq[c, x] = total.astype(BF16)
    x_all = {
        d: send(pq.at[c, x], pq.at[c, x], xg_s.at[d], xg_r.at[d], at_x(d)) for d in (2, 1, 3)
    }
    passed = [send(pq.at[c, x], pq.at[c, x], fw_s.at[0], fw_r.at[0], partner)]

    for s in (1, 2):
        for h in (0, 1):
            ring_wait(s, h)
            ring_step(s + 1, h)

    for d in (1, 3, 2):
        x_all[d].wait_recv()
        xx = lax.rem(x + X - d, X)
        passed.append(send(pq.at[c, xx], pq.at[c, xx], fw_s.at[d], fw_r.at[d], partner))
    loads["vc"].wait()
    pq_mine = pq[c].reshape(256, 512)
    lv = rows_dot(pq_mine[:, :RANK], vc_v[mine])
    lo = rows_dot(pq_mine[:, RANK:], heads[mine])
    for copy in passed:
        copy.wait_recv()
    pq_theirs = pq[1 - c].reshape(256, 512)
    lv += rows_dot(pq_theirs[:, :RANK], vc_v[theirs])
    lo += rows_dot(pq_theirs[:, RANK:], heads[theirs])
    scale = 1.0 / math.sqrt(32768.0)
    lv3 = (lv * scale).reshape(32, 8, 256)
    lo3 = (lo * scale).reshape(32, 8, 256)
    upper = lax.broadcasted_iota(jnp.int32, (32, 8, 256), 1) < 4
    even = jnp.where(upper, lv3, pltpu.roll(lo3, 4, 1)).astype(BF16)
    odd = jnp.where(upper, pltpu.roll(lv3, 4, 1), lo3).astype(BF16)
    for f in range(Z * Y):
        block = (odd if f % 2 else even)[f // 2]
        la[f // Y, f % Y] = block[:, :128]
        lb[f % Y, f // Y] = block[:, 128:]
    r1a, r1b = {}, {}
    for d in FAR:
        r1a[d] = send(la.at[lax.rem(z + d, Z)], ra.at[z], r1a_s.at[d], r1a_r.at[d], at_z(d))
        r1b[d] = send(lb.at[lax.rem(y + d, Y)], rb.at[y], r1b_s.at[d], r1b_r.at[d], at_y(d))

    open_group(z)
    open_group(lax.rem(z + Z - 1, Z))
    open_group(lax.rem(z + 1, Z))
    ring_wait(3, 0)
    ring_step(4, 0)
    ring_wait(3, 1)
    ring_step(4, 1)
    open_group(lax.rem(z + Z - 2, Z))
    open_group(lax.rem(z + 2, Z))
    open_group(lax.rem(z + Z - 3, Z))
    open_group(lax.rem(z + 3, Z))
    ring_wait(4, 0)
    ring_wait(4, 1)
    open_group(lax.rem(z + 4, Z))

    sum_a = la[z].astype(F32)
    sum_b = lb[y].astype(F32)
    for d in NEAR:
        r1a[d].wait_recv()
        sum_a += ra[lax.rem(z + Z - d, Z)].astype(F32)
        r1b[d].wait_recv()
        sum_b += rb[lax.rem(y + Y - d, Y)].astype(F32)
    sa[...] = sum_a
    sb[...] = sum_b
    r2a, r2b = {}, {}
    for d in FAR:
        r2a[d] = send(sa.at[lax.rem(y + d, Y)], ra2.at[y], r2a_s.at[d], r2a_r.at[d], at_y(d))
        r2b[d] = send(sb.at[lax.rem(z + d, Z)], rb2.at[z], r2b_s.at[d], r2b_r.at[d], at_z(d))

    for k in range(Z // 2):
        wo_f[:, k * 256 : (k + 1) * 256] = decode(wo[k].reshape(256, 256).T, WEIGHT_RATE)

    low_a = sa[y]
    low_b = sb[z]
    for d in NEAR:
        r2a[d].wait_recv()
        low_a += ra2[lax.rem(y + Y - d, Y)]
        r2b[d].wait_recv()
        low_b += rb2[lax.rem(z + Z - d, Z)]
    low = jnp.concatenate([low_a, low_b], axis=1)
    low_v[...] = low
    for name in ("vm", "om", "vs", "os"):
        loads[name].wait()
    moment = 0.8 * mom_v[...] + 0.2 * low
    spread = 0.95 * sec_v[...] + 0.05 * low * low
    code = encode(moment / (jnp.sqrt(spread) + 1e-08), DIRECTION_RATE)
    da[z, y] = code[:, :128]
    db[y, z] = code[:, 128:]
    g1a, g1b, g2a, g2b = {}, {}, {}, {}
    for d in FAR:
        g1a[d] = send(da.at[z, y], da.at[z, y], g1a_s.at[d], g1a_r.at[d], at_y(d))
        g1b[d] = send(db.at[y, z], db.at[y, z], g1b_s.at[d], g1b_r.at[d], at_z(d))

    for k in range(Z // 2, Z):
        wo_f[:, k * 256 : (k + 1) * 256] = decode(wo[k].reshape(256, 256).T, WEIGHT_RATE)
    for d in NEAR:
        g1a[d].wait_recv()
    for d in FAR:
        g2a[d] = send(da.at[z], da.at[z], g2a_s.at[d], g2a_r.at[d], at_z(d))
    for d in NEAR:
        g1b[d].wait_recv()
    for d in FAR:
        g2b[d] = send(db.at[y], db.at[y], g2b_s.at[d], g2b_r.at[d], at_y(d))
    for d in NEAR:
        g2a[d].wait_recv()
        g2b[d].wait_recv()
    sent = to_pair + passed
    for group in (w1v, w1o, x_sum, x_all, r1a, r1b, r2a, r2b, g1a, g1b, g2a, g2b):
        sent += list(group.values())
    for ring in rings.values():
        sent += ring
    for copy in sent:
        copy.wait_send()


def finish_kernel(
    da, db, wv, wo, low, vf, of, vw, ow, vm, vs, om, os_,
    vmaster, omaster, vm_new, vs_new, om_new, os_new, vcopy, ocopy,
    dv, do, do_t, vc_v, oc_v, n_v, k_v, out_sem, chunk_sem,
):
    fs = lax.axis_index("fs")
    upper = lax.broadcasted_iota(jnp.int32, (8, 256), 0) < 4
    for g in range(Z * Y // 2):
        zz, yy = (2 * g) // Y, (2 * g) % Y
        even = jnp.concatenate([da[zz, yy], db[yy, zz]], axis=1)
        odd = jnp.concatenate([da[zz, yy + 1], db[yy + 1, zz]], axis=1)
        even = 0.05 * decode(even, DIRECTION_RATE)
        odd = 0.05 * decode(odd, DIRECTION_RATE)
        value = jnp.where(upper, even, pltpu.roll(odd, 4, 0))
        output = jnp.where(upper, pltpu.roll(even, 4, 0), odd)
        for full, both in ((value, dv), (output, do)):
            top = full.astype(BF16)
            both[8 * g : 8 * g + 8] = top
            both[RANK + 8 * g : RANK + 8 * g + 8] = (full - top.astype(F32)).astype(BF16)
    do_t[...] = do[...].T
    outs = []

    def put(src, dst, sem):
        copy = pltpu.make_async_copy(src, dst, sem)
        copy.start()
        outs.append(copy)

    for k in range(CHUNKS):
        rows = pl.ds(k * STEP, STEP)
        factor = vf[rows]
        step = jnp.dot(
            jnp.concatenate([factor, factor], axis=1), dv[...], preferred_element_type=F32
        )
        vc_v[rows] = (wv[rows] - step).astype(BF16)
        put(vc_v.at[rows], vcopy.at[rows], chunk_sem.at[k])
    for k in range(CHUNKS):
        rows = pl.ds(k * STEP, STEP)
        factor = of[rows]
        step = lax.dot_general(
            do_t[...],
            jnp.concatenate([factor, factor], axis=1),
            (((1,), (1,)), ((), ())),
            preferred_element_type=F32,
        )
        oc_v[:, rows] = (wo[:, rows] - step).astype(BF16)
        put(oc_v.at[:, rows], ocopy.at[:, rows], chunk_sem.at[CHUNKS + k])
        if k == 0:
            low_v, low_o = low[0:4], low[4:8]
            n_v[0] = 0.8 * vm[...] + 0.2 * low_v
            n_v[1] = 0.95 * vs[...] + 0.05 * low_v * low_v
            n_v[2] = 0.8 * om[...] + 0.2 * low_o
            n_v[3] = 0.95 * os_[...] + 0.05 * low_o * low_o
            for i, dst in enumerate((vm_new, vs_new, om_new, os_new)):
                put(n_v.at[i], dst, out_sem.at[i])
    own = pl.ds(pl.multiple_of(fs * WIDTH_ROWS, WIDTH_ROWS), WIDTH_ROWS)
    for i, (factor, both, weight, out) in enumerate(
        ((vf, dv, vw, vmaster), (of, do, ow, omaster))
    ):
        rows = factor[own]
        k_v[i] = weight[...] - jnp.dot(
            jnp.concatenate([rows, rows], axis=1), both[...], preferred_element_type=F32
        )
        put(k_v.at[i], out, out_sem.at[4 + i])
    for copy in outs:
        copy.wait()


def local(
    inputs, value_cotangent, first_map, second_map, lambdas, head_gain, output_cotangent,
    value_factor, output_factor, value_weight, output_weight,
    value_moment, value_second, output_moment, output_second,
):
    turned_weight = output_weight.T
    gain = head_gain.reshape(1, HEAD)
    hbm = pl.BlockSpec(memory_space=pltpu.HBM)
    near = pl.BlockSpec(memory_space=pltpu.VMEM)
    dma = pltpu.SemaphoreType.DMA
    vmem = pltpu.VMEM
    sems = [dma((13,)), dma((2,)), dma((2,)), dma((4,)), dma((4,)), dma((4,)), dma((4,)), dma((4,)), dma((4,))]
    sems += [dma((8,))] * 20 + [dma((16,))] * 4
    far = [
        pltpu.with_memory_space_constraint(a, pltpu.HBM)
        for a in (
            inputs, output_cotangent, value_cotangent, first_map, second_map, lambdas, gain,
            value_factor, output_factor, value_weight, turned_weight,
            value_moment, value_second, output_moment, output_second,
        )
    ]
    wv, wo, da, db, low = pl.pallas_call(
        exchange_kernel,
        out_shape=[
            jax.ShapeDtypeStruct((Z, 256, 256), F32),
            jax.ShapeDtypeStruct((256, 2048), F32),
            jax.ShapeDtypeStruct((Z, Y, 8, 128), BF16),
            jax.ShapeDtypeStruct((Y, Z, 8, 128), BF16),
            jax.ShapeDtypeStruct((8, 256), F32),
        ],
        in_specs=[hbm] * 5
        + [pl.BlockSpec(memory_space=pltpu.SMEM), pl.BlockSpec(memory_space=pltpu.VMEM)]
        + [hbm] * 8,
        out_specs=[near] * 5,
        scratch_shapes=[
            vmem((512, 256), BF16), vmem((512, 256), BF16), vmem((512, 256), BF16),
            vmem((512, 256), BF16), vmem((512, 256), BF16),
            vmem((512, 256), BF16), vmem((512, 256), BF16),
            vmem((WIDTH_ROWS, 256), F32), vmem((WIDTH_ROWS, 256), F32),
            vmem((8, 256), F32), vmem((8, 256), F32),
            vmem((2, 256, 256), BF16), vmem((X, 64, 512), F32), vmem((X, 64, 512), BF16),
            vmem((X, 64, 512), BF16), vmem((C, X, 64, 512), BF16), vmem((512, 256), BF16),
            vmem((Z, Y, 8, 128), BF16), vmem((Y, Z, 8, 128), BF16),
            vmem((Z, Y, 8, 128), BF16), vmem((Y, Z, 8, 128), BF16),
            vmem((Y, 8, 128), F32), vmem((Z, 8, 128), F32),
            vmem((Y, 8, 128), F32), vmem((Z, 8, 128), F32),
            vmem((Z, Y, WIDTH_ROWS, 256), BF16), vmem((Z, Y, WIDTH_ROWS, 256), BF16),
        ]
        + sems,
        compiler_params=pltpu.CompilerParams(
            collective_id=0, has_side_effects=True, vmem_limit_bytes=24 * 1024 * 1024
        ),
        name="exchange",
    )(*far)
    width, cols = 2048, 256
    wv = wv.reshape(width, cols)

    small = jax.ShapeDtypeStruct((4, cols), F32)
    own = jax.ShapeDtypeStruct((WIDTH_ROWS, cols), F32)
    vmaster, omaster, *rest = pl.pallas_call(
        finish_kernel,
        out_shape=[
            own, own, small, small, small, small,
            jax.ShapeDtypeStruct((width, cols), BF16),
            jax.ShapeDtypeStruct((cols, width), BF16),
        ],
        in_specs=[near] * 13,
        out_specs=[hbm] * 8,
        scratch_shapes=[
            vmem((2 * RANK, cols), BF16), vmem((2 * RANK, cols), BF16), vmem((cols, 2 * RANK), BF16),
            vmem((width, cols), BF16), vmem((cols, width), BF16),
            vmem((4, 4, cols), F32), vmem((2, WIDTH_ROWS, cols), F32),
            dma((6,)), dma((2 * CHUNKS,)),
        ],
        compiler_params=pltpu.CompilerParams(vmem_limit_bytes=24 * 1024 * 1024),
        name="finish",
    )(
        da, db, wv, wo, low, value_factor, output_factor, value_weight, turned_weight,
        value_moment, value_second, output_moment, output_second,
    )
    return (vmaster, omaster.T, *rest)


def solution(mesh):
    both = P("fs", "tp")
    in_specs = (
        both, both, both, both, P("tp"), P(), both, P(), P(), both, P("tp", "fs"),
        both, both, both, both,
    )
    out_specs = (
        both, P("tp", "fs"), both, both, both, both, P(None, "tp"), P("tp", None),
    )
    return jax.shard_map(local, mesh=mesh, in_specs=in_specs, out_specs=out_specs, check_vma=False)
```

time: 62.5 us -> 59.6 us (0.954)
  Pallas kernels: 61.5 us -> 58.7 us
    pallas_call x1, Pallas kernels: 6.27 us -> 2.42 us  [local(): pl.pallas_call(finish_kernel, out_shape=[own, own, small, small, small, s...]
    pallas_call x1, Pallas kernels: 55.2 us -> 56.2 us  [local(): pl.pallas_call(exchange_kernel, out_shape=[jax.ShapeDtypeStruct((Z, 256,...]
where the time goes in v3:
time: 59.6 us; the launch traced here: 59.5 us
  Pallas kernels  58.7 us (98%)
  between operations  0.77 us (1%)
    pallas_call x1, Pallas kernels, local(): pl.pallas_call(exchange_kernel, out_shape=[jax.ShapeDtypeStruct((Z, 256,...  56.2 us
    pallas_call x1, Pallas kernels, local(): pl.pallas_call(finish_kernel, out_shape=[own, own, small, small, small, s...  2.42 us

profile of v3, /device:TPU:6, one launch (start us, length us, event | category | flops | bytes accessed | tf_op | source)
XLA Modules:
  0.0 59.5 jit_solution(14871396208248544741)
XLA Ops:
  0.6 0.0 copy-start.7
  0.6 0.0 copy-start.6
  0.7 0.0 copy-start.5
  0.7 0.0 copy-start.4
  0.7 0.0 copy-start.2
  0.7 0.0 copy-start.1
  0.7 0.0 copy-start
  0.7 0.0 copy-start.3
  0.7 56.2 %exchange.1 = (f32[8,256,256]{2,1,0:T(8,128)S(1)}, f32[256,2048]{1,0:T(8,128)S(1)}, bf16[8,8,8,128]{3,2,1,0:T(8,128)(2,1)S(1)}, bf16[8,8,8,128]{3,2,1,0:T(8,128)(2,1)S(1)}, f32[8,256]{1,0:T(8,128)S(1)}) custom-call(bf16[512,256]{1,0:T(8,128)(2,1)} %inputs.1, bf16[512,256]{1,0:T(8,128)(2,1)} %ocot.1, bf16[512,256]{1,0:T(8,128)(2,1)} %vcot.1, ...), custom_call_target="tpu_custom_call" | custom-call | tf_op jit(solution)/shard_map/exchange/pallas_call | solution.py:380
  57.0 0.0 copy-done.7
  57.0 0.0 copy-done.6
  57.0 0.0 copy-done.5
  57.0 0.0 copy-done.4
  57.0 0.0 copy-done.2
  57.0 0.0 copy-done.1
  57.0 0.0 copy-done
  57.0 0.0 copy-done.3
  57.0 2.4 %finish.1 = (f32[32,256]{1,0:T(8,128)}, f32[32,256]{1,0:T(8,128)}, f32[4,256]{1,0:T(4,128)}, f32[4,256]{1,0:T(4,128)}, f32[4,256]{1,0:T(4,128)}, /*index=5*/f32[...) custom-call(bf16[8,8,8,128]{3,2,1,0:T(8,128)(2,1)S(1)} %get-tuple-element.21.da, ...), custom_call_target="tpu_custom_call" | custom-call | tf_op jit(solution)/shard_map/finish/pallas_call | solution.py:418
Async XLA Ops:
  0.6 56.3 %copy-start.7 = (f32[4,256]{1,0:T(4,128)S(1)}, f32[4,256]{1,0:T(4,128)}, u32[]{:S(2)}) copy-start(f32[4,256]{1,0:T(4,128)} %os_.3) | copy-start | bytes 12292
  0.6 56.3 %copy-start.6 = (f32[4,256]{1,0:T(4,128)S(1)}, f32[4,256]{1,0:T(4,128)}, u32[]{:S(2)}) copy-start(f32[4,256]{1,0:T(4,128)} %om.3) | copy-start | bytes 12292
  0.7 56.3 %copy-start.5 = (f32[4,256]{1,0:T(4,128)S(1)}, f32[4,256]{1,0:T(4,128)}, u32[]{:S(2)}) copy-start(f32[4,256]{1,0:T(4,128)} %vs.3) | copy-start | bytes 12292
  0.7 56.3 %copy-start.4 = (f32[4,256]{1,0:T(4,128)S(1)}, f32[4,256]{1,0:T(4,128)}, u32[]{:S(2)}) copy-start(f32[4,256]{1,0:T(4,128)} %vm.3) | copy-start | bytes 12292
  0.7 56.3 %copy-start.2 = (f32[32,256]{1,0:T(8,128)S(1)}, f32[32,256]{1,0:T(8,128)}, u32[]{:S(2)}) copy-start(f32[32,256]{1,0:T(8,128)} %vw.3) | copy-start | bytes 98308
  0.7 56.3 %copy-start.1 = (bf16[2048,256]{1,0:T(8,128)(2,1)S(1)}, bf16[2048,256]{1,0:T(8,128)(2,1)}, u32[]{:S(2)}) copy-start(bf16[2048,256]{1,0:T(8,128)(2,1)} %of.3) | copy-start | bytes 3145732
  0.7 56.3 %copy-start = (bf16[2048,256]{1,0:T(8,128)(2,1)S(1)}, bf16[2048,256]{1,0:T(8,128)(2,1)}, u32[]{:S(2)}) copy-start(bf16[2048,256]{1,0:T(8,128)(2,1)} %vf.3) | copy-start | bytes 3145732
  0.7 56.3 %copy-start.3 = (f32[256,32]{0,1:T(8,128)S(1)}, f32[256,32]{0,1:T(8,128)}, u32[]{:S(2)}) copy-start(f32[256,32]{0,1:T(8,128)} %param.25) | copy-start | bytes 98308

commit v4 on v3

--- a/solution.py
+++ b/solution.py
@@ -181,10 +181,10 @@
     }
     passed = [send(pq.at[c, x], pq.at[c, x], fw_s.at[0], fw_r.at[0], partner)]
 
-    for s in (1, 2):
-        for h in (0, 1):
-            ring_wait(s, h)
-            ring_step(s + 1, h)
+    ring_wait(1, 0)
+    ring_step(2, 0)
+    ring_wait(1, 1)
+    ring_step(2, 1)
 
     for d in (1, 3, 2):
         x_all[d].wait_recv()
@@ -214,21 +214,13 @@
         r1a[d] = send(la.at[lax.rem(z + d, Z)], ra.at[z], r1a_s.at[d], r1a_r.at[d], at_z(d))
         r1b[d] = send(lb.at[lax.rem(y + d, Y)], rb.at[y], r1b_s.at[d], r1b_r.at[d], at_y(d))
 
+    ring_wait(2, 0)
+    ring_step(3, 0)
+    ring_wait(2, 1)
+    ring_step(3, 1)
     open_group(z)
     open_group(lax.rem(z + Z - 1, Z))
     open_group(lax.rem(z + 1, Z))
-    ring_wait(3, 0)
-    ring_step(4, 0)
-    ring_wait(3, 1)
-    ring_step(4, 1)
-    open_group(lax.rem(z + Z - 2, Z))
-    open_group(lax.rem(z + 2, Z))
-    open_group(lax.rem(z + Z - 3, Z))
-    open_group(lax.rem(z + 3, Z))
-    ring_wait(4, 0)
-    ring_wait(4, 1)
-    open_group(lax.rem(z + 4, Z))
-
     sum_a = la[z].astype(F32)
     sum_b = lb[y].astype(F32)
     for d in NEAR:
@@ -243,8 +235,12 @@
         r2a[d] = send(sa.at[lax.rem(y + d, Y)], ra2.at[y], r2a_s.at[d], r2a_r.at[d], at_y(d))
         r2b[d] = send(sb.at[lax.rem(z + d, Z)], rb2.at[z], r2b_s.at[d], r2b_r.at[d], at_z(d))
 
-    for k in range(Z // 2):
-        wo_f[:, k * 256 : (k + 1) * 256] = decode(wo[k].reshape(256, 256).T, WEIGHT_RATE)
+    ring_wait(3, 0)
+    ring_step(4, 0)
+    ring_wait(3, 1)
+    ring_step(4, 1)
+    open_group(lax.rem(z + Z - 2, Z))
+    open_group(lax.rem(z + 2, Z))
 
     low_a = sa[y]
     low_b = sb[z]
@@ -267,7 +263,12 @@
         g1a[d] = send(da.at[z, y], da.at[z, y], g1a_s.at[d], g1a_r.at[d], at_y(d))
         g1b[d] = send(db.at[y, z], db.at[y, z], g1b_s.at[d], g1b_r.at[d], at_z(d))
 
-    for k in range(Z // 2, Z):
+    ring_wait(4, 0)
+    ring_wait(4, 1)
+    open_group(lax.rem(z + 4, Z))
+    open_group(lax.rem(z + Z - 3, Z))
+    open_group(lax.rem(z + 3, Z))
+    for k in range(Z):
         wo_f[:, k * 256 : (k + 1) * 256] = decode(wo[k].reshape(256, 256).T, WEIGHT_RATE)
     for d in NEAR:
         g1a[d].wait_recv()

time: 59.6 us -> 53.7 us (0.901)
  Pallas kernels: 58.7 us -> 52.4 us
    pallas_call x1, Pallas kernels: 56.2 us -> 50 us  [local(): pl.pallas_call(exchange_kernel, out_shape=[jax.ShapeDtypeStruct((Z, 256,...]
where the time goes in v4:
time: 53.7 us; the launch traced here: 53.2 us
  Pallas kernels  52.4 us (98%)
  between operations  0.77 us (1%)
    pallas_call x1, Pallas kernels, local(): pl.pallas_call(exchange_kernel, out_shape=[jax.ShapeDtypeStruct((Z, 256,...  50 us
    pallas_call x1, Pallas kernels, local(): pl.pallas_call(finish_kernel, out_shape=[own, own, small, small, small, s...  2.42 us

profile of v4, /device:TPU:6, one launch (start us, length us, event | category | flops | bytes accessed | tf_op | source)
XLA Modules:
  0.0 53.2 jit_solution(7858016064725421356)
XLA Ops:
  0.6 0.0 copy-start.7
  0.6 0.0 copy-start.6
  0.7 0.0 copy-start.5
  0.7 0.0 copy-start.4
  0.7 0.0 copy-start.2
  0.7 0.0 copy-start.1
  0.7 0.0 copy-start
  0.7 0.0 copy-start.3
  0.7 50.0 %exchange.1 = (f32[8,256,256]{2,1,0:T(8,128)S(1)}, f32[256,2048]{1,0:T(8,128)S(1)}, bf16[8,8,8,128]{3,2,1,0:T(8,128)(2,1)S(1)}, bf16[8,8,8,128]{3,2,1,0:T(8,128)(2,1)S(1)}, f32[8,256]{1,0:T(8,128)S(1)}) custom-call(bf16[512,256]{1,0:T(8,128)(2,1)} %inputs.1, bf16[512,256]{1,0:T(8,128)(2,1)} %ocot.1, bf16[512,256]{1,0:T(8,128)(2,1)} %vcot.1, ...), custom_call_target="tpu_custom_call" | custom-call | tf_op jit(solution)/shard_map/exchange/pallas_call | solution.py:381
  50.7 0.0 copy-done.7
  50.7 0.0 copy-done.6
  50.7 0.0 copy-done.5
  50.7 0.0 copy-done.4
  50.7 0.0 copy-done.2
  50.7 0.0 copy-done.1
  50.7 0.0 copy-done
  50.8 0.0 copy-done.3
  50.8 2.4 %finish.1 = (f32[32,256]{1,0:T(8,128)}, f32[32,256]{1,0:T(8,128)}, f32[4,256]{1,0:T(4,128)}, f32[4,256]{1,0:T(4,128)}, f32[4,256]{1,0:T(4,128)}, /*index=5*/f32[...) custom-call(bf16[8,8,8,128]{3,2,1,0:T(8,128)(2,1)S(1)} %get-tuple-element.21.da, ...), custom_call_target="tpu_custom_call" | custom-call | tf_op jit(solution)/shard_map/finish/pallas_call | solution.py:419
Async XLA Ops:
  0.6 50.0 %copy-start.7 = (f32[4,256]{1,0:T(4,128)S(1)}, f32[4,256]{1,0:T(4,128)}, u32[]{:S(2)}) copy-start(f32[4,256]{1,0:T(4,128)} %os_.3) | copy-start | bytes 12292
  0.6 50.0 %copy-start.6 = (f32[4,256]{1,0:T(4,128)S(1)}, f32[4,256]{1,0:T(4,128)}, u32[]{:S(2)}) copy-start(f32[4,256]{1,0:T(4,128)} %om.3) | copy-start | bytes 12292
  0.7 50.0 %copy-start.5 = (f32[4,256]{1,0:T(4,128)S(1)}, f32[4,256]{1,0:T(4,128)}, u32[]{:S(2)}) copy-start(f32[4,256]{1,0:T(4,128)} %vs.3) | copy-start | bytes 12292
  0.7 50.0 %copy-start.4 = (f32[4,256]{1,0:T(4,128)S(1)}, f32[4,256]{1,0:T(4,128)}, u32[]{:S(2)}) copy-start(f32[4,256]{1,0:T(4,128)} %vm.3) | copy-start | bytes 12292
  0.7 50.0 %copy-start.2 = (f32[32,256]{1,0:T(8,128)S(1)}, f32[32,256]{1,0:T(8,128)}, u32[]{:S(2)}) copy-start(f32[32,256]{1,0:T(8,128)} %vw.3) | copy-start | bytes 98308
  0.7 50.0 %copy-start.1 = (bf16[2048,256]{1,0:T(8,128)(2,1)S(1)}, bf16[2048,256]{1,0:T(8,128)(2,1)}, u32[]{:S(2)}) copy-start(bf16[2048,256]{1,0:T(8,128)(2,1)} %of.3) | copy-start | bytes 3145732
  0.7 50.0 %copy-start = (bf16[2048,256]{1,0:T(8,128)(2,1)S(1)}, bf16[2048,256]{1,0:T(8,128)(2,1)}, u32[]{:S(2)}) copy-start(bf16[2048,256]{1,0:T(8,128)(2,1)} %vf.3) | copy-start | bytes 3145732
  0.7 50.0 %copy-start.3 = (f32[256,32]{0,1:T(8,128)S(1)}, f32[256,32]{0,1:T(8,128)}, u32[]{:S(2)}) copy-start(f32[256,32]{0,1:T(8,128)} %param.25) | copy-start | bytes 98308

commit v5 on v4

--- a/solution.py
+++ b/solution.py
@@ -39,7 +39,7 @@
 def exchange_kernel(
     inputs, ocot, vcot, first, second, lambdas, gain, vf, of, vw, ow, vm, vs, om, os_,
     wv_f, wo_f, da, db, low_v,
-    in_v, oc_v, vc_v, fi_v, se_v, vf_v, of_v, vw_v, ow_v, mom_v, sec_v,
+    in_v, oc_v, vc_v, fi_v, se_v, vf_v, of_v, vw_v, ow_v, ma, mb,
     pair, ax, sx, rx, pq, heads,
     la, lb, ra, rb, sa, sb, ra2, rb2, wv, wo,
     load_sem,
@@ -91,10 +91,13 @@
             ("fi", first, fi_v),
             ("se", second, se_v),
             ("vc", vcot, vc_v),
-            ("vm", vm, mom_v.at[pl.ds(0, 4)]),
-            ("om", om, mom_v.at[pl.ds(4, 4)]),
-            ("vs", vs, sec_v.at[pl.ds(0, 4)]),
-            ("os", os_, sec_v.at[pl.ds(4, 4)]),
+        ]
+        + [
+            (f"{name}{i}", src.at[:, pl.ds(i * 128, 128)], dst.at[kind, pl.ds(row, 4)])
+            for i, dst in enumerate((ma.at[y], mb.at[z]))
+            for name, src, kind, row in (
+                ("vm", vm, 0, 0), ("om", om, 0, 4), ("vs", vs, 1, 0), ("os", os_, 1, 4)
+            )
         ]
     ):
         loads[name] = pltpu.make_async_copy(src, dst, load_sem.at[i])
@@ -117,19 +120,26 @@
         w1o[d] = send(wo.at[z, y], wo.at[z, y], w1o_s.at[d], w1o_r.at[d], at_z(d))
     for name in ("in", "vf", "oc", "of"):
         loads[name].wait()
-    acc_p = jnp.dot(in_v[mine], vf_v[mine], preferred_element_type=F32)
-    acc_q = jnp.dot(oc_v[mine], of_v[mine], preferred_element_type=F32)
     for copy in to_pair:
         copy.wait_recv()
-    acc_p += jnp.dot(pair[0], vf_v[theirs], preferred_element_type=F32)
-    acc_q += jnp.dot(pair[1], of_v[theirs], preferred_element_type=F32)
-    acc = jnp.concatenate([acc_p, acc_q], axis=1).reshape(X, 64, 512)
-    ax[...] = acc
-    sx[...] = acc.astype(BF16)
-    x_sum = {
-        d: send(sx.at[lax.rem(x + d, X)], rx.at[x], xs_s.at[d], xs_r.at[d], at_x(d))
-        for d in (2, 1, 3)
-    }
+    x_sum = {}
+    for h in range(2):
+
+        def part(tokens):
+            return tokens.reshape(X, 64, 256)[:, h * 32 : (h + 1) * 32].reshape(X * 32, 256)
+
+        acc_p = jnp.dot(part(in_v[mine]), vf_v[mine], preferred_element_type=F32)
+        acc_q = jnp.dot(part(oc_v[mine]), of_v[mine], preferred_element_type=F32)
+        acc_p += jnp.dot(part(pair[0]), vf_v[theirs], preferred_element_type=F32)
+        acc_q += jnp.dot(part(pair[1]), of_v[theirs], preferred_element_type=F32)
+        acc = jnp.concatenate([acc_p, acc_q], axis=1).reshape(X, 32, 512)
+        ax[h] = acc
+        sx[h] = acc.astype(BF16)
+        for d in (2, 1, 3):
+            k = 4 * h + d
+            x_sum[h, d] = send(
+                sx.at[h, lax.rem(x + d, X)], rx.at[h, x], xs_s.at[k], xs_r.at[k], at_x(d)
+            )
 
     def ring_step(s, h):
         half = pl.ds(h * 4, 4)
@@ -160,6 +170,13 @@
     for d in NEAR:
         w1v[d].wait_recv()
         w1o[d].wait_recv()
+    for name in ("vm", "om", "vs", "os"):
+        loads[name + "0"].wait()
+        loads[name + "1"].wait()
+    g1a, g1b = {}, {}
+    for d in FAR:
+        g1a[d] = send(ma.at[y], ma.at[y], g1a_s.at[d], g1a_r.at[d], at_y(d))
+        g1b[d] = send(mb.at[z], mb.at[z], g1b_s.at[d], g1b_r.at[d], at_z(d))
     ring_step(1, 0)
     ring_step(1, 1)
 
@@ -171,25 +188,30 @@
         mean = jnp.mean(difference * difference, axis=-1, keepdims=True)
         heads[:, cols] = (difference * lax.rsqrt(mean + 1e-06) * gain[...]).astype(BF16)
 
-    total = ax[x]
-    for d in (1, 3, 2):
-        x_sum[d].wait_recv()
-        total += rx[lax.rem(x + X - d, X)].astype(F32)
-    pq[c, x] = total.astype(BF16)
-    x_all = {
-        d: send(pq.at[c, x], pq.at[c, x], xg_s.at[d], xg_r.at[d], at_x(d)) for d in (2, 1, 3)
-    }
-    passed = [send(pq.at[c, x], pq.at[c, x], fw_s.at[0], fw_r.at[0], partner)]
+    x_all, passed = {}, []
+    for h in range(2):
+        total = ax[h, x]
+        for d in (1, 3, 2):
+            x_sum[h, d].wait_recv()
+            total += rx[h, lax.rem(x + X - d, X)].astype(F32)
+        pq[c, x, h] = total.astype(BF16)
+        block = pq.at[c, x, h]
+        for d in (2, 1, 3):
+            k = 4 * h + d
+            x_all[h, d] = send(block, block, xg_s.at[k], xg_r.at[k], at_x(d))
+        passed.append(send(block, block, fw_s.at[4 * h], fw_r.at[4 * h], partner))
 
     ring_wait(1, 0)
     ring_step(2, 0)
     ring_wait(1, 1)
     ring_step(2, 1)
 
-    for d in (1, 3, 2):
-        x_all[d].wait_recv()
-        xx = lax.rem(x + X - d, X)
-        passed.append(send(pq.at[c, xx], pq.at[c, xx], fw_s.at[d], fw_r.at[d], partner))
+    for h in range(2):
+        for d in (1, 3, 2):
+            x_all[h, d].wait_recv()
+            block = pq.at[c, lax.rem(x + X - d, X), h]
+            k = 4 * h + d
+            passed.append(send(block, block, fw_s.at[k], fw_r.at[k], partner))
     loads["vc"].wait()
     pq_mine = pq[c].reshape(256, 512)
     lv = rows_dot(pq_mine[:, :RANK], vc_v[mine])
@@ -228,12 +250,12 @@
         sum_a += ra[lax.rem(z + Z - d, Z)].astype(F32)
         r1b[d].wait_recv()
         sum_b += rb[lax.rem(y + Y - d, Y)].astype(F32)
-    sa[...] = sum_a
-    sb[...] = sum_b
+    ra2[y] = sum_a.astype(BF16)
+    rb2[z] = sum_b.astype(BF16)
     r2a, r2b = {}, {}
     for d in FAR:
-        r2a[d] = send(sa.at[lax.rem(y + d, Y)], ra2.at[y], r2a_s.at[d], r2a_r.at[d], at_y(d))
-        r2b[d] = send(sb.at[lax.rem(z + d, Z)], rb2.at[z], r2b_s.at[d], r2b_r.at[d], at_z(d))
+        r2a[d] = send(ra2.at[y], ra2.at[y], r2a_s.at[d], r2a_r.at[d], at_y(d))
+        r2b[d] = send(rb2.at[z], rb2.at[z], r2b_s.at[d], r2b_r.at[d], at_z(d))
 
     ring_wait(3, 0)
     ring_step(4, 0)
@@ -241,43 +263,39 @@
     ring_step(4, 1)
     open_group(lax.rem(z + Z - 2, Z))
     open_group(lax.rem(z + 2, Z))
-
-    low_a = sa[y]
-    low_b = sb[z]
+    open_group(lax.rem(z + Z - 3, Z))
+    open_group(lax.rem(z + 3, Z))
+    for d in NEAR:
+        g1a[d].wait_recv()
+        g1b[d].wait_recv()
+
+    def directions(sums, moments, lows):
+        low = sums[0].astype(F32)
+        for k in range(1, 8):
+            low += sums[k].astype(F32)
+        lows[...] = low
+        moment = 0.8 * moments[:, 0] + 0.2 * low
+        spread = 0.95 * moments[:, 1] + 0.05 * low * low
+        return encode(moment / (jnp.sqrt(spread) + 1e-08), DIRECTION_RATE)
+
+    g2a, g2b = {}, {}
     for d in NEAR:
         r2a[d].wait_recv()
-        low_a += ra2[lax.rem(y + Y - d, Y)]
+    da[z] = directions(ra2, ma, sa)
+    for d in FAR:
+        g2a[d] = send(da.at[z], da.at[z], g2a_s.at[d], g2a_r.at[d], at_z(d))
+    for d in NEAR:
         r2b[d].wait_recv()
-        low_b += rb2[lax.rem(z + Z - d, Z)]
-    low = jnp.concatenate([low_a, low_b], axis=1)
-    low_v[...] = low
-    for name in ("vm", "om", "vs", "os"):
-        loads[name].wait()
-    moment = 0.8 * mom_v[...] + 0.2 * low
-    spread = 0.95 * sec_v[...] + 0.05 * low * low
-    code = encode(moment / (jnp.sqrt(spread) + 1e-08), DIRECTION_RATE)
-    da[z, y] = code[:, :128]
-    db[y, z] = code[:, 128:]
-    g1a, g1b, g2a, g2b = {}, {}, {}, {}
-    for d in FAR:
-        g1a[d] = send(da.at[z, y], da.at[z, y], g1a_s.at[d], g1a_r.at[d], at_y(d))
-        g1b[d] = send(db.at[y, z], db.at[y, z], g1b_s.at[d], g1b_r.at[d], at_z(d))
+    db[y] = directions(rb2, mb, sb)
+    for d in FAR:
+        g2b[d] = send(db.at[y], db.at[y], g2b_s.at[d], g2b_r.at[d], at_y(d))
+    low_v[...] = jnp.concatenate([sa[y], sb[z]], axis=1)
 
     ring_wait(4, 0)
     ring_wait(4, 1)
     open_group(lax.rem(z + 4, Z))
-    open_group(lax.rem(z + Z - 3, Z))
-    open_group(lax.rem(z + 3, Z))
     for k in range(Z):
         wo_f[:, k * 256 : (k + 1) * 256] = decode(wo[k].reshape(256, 256).T, WEIGHT_RATE)
-    for d in NEAR:
-        g1a[d].wait_recv()
-    for d in FAR:
-        g2a[d] = send(da.at[z], da.at[z], g2a_s.at[d], g2a_r.at[d], at_z(d))
-    for d in NEAR:
-        g1b[d].wait_recv()
-    for d in FAR:
-        g2b[d] = send(db.at[y], db.at[y], g2b_s.at[d], g2b_r.at[d], at_y(d))
     for d in NEAR:
         g2a[d].wait_recv()
         g2b[d].wait_recv()
@@ -368,7 +386,7 @@
     near = pl.BlockSpec(memory_space=pltpu.VMEM)
     dma = pltpu.SemaphoreType.DMA
     vmem = pltpu.VMEM
-    sems = [dma((13,)), dma((2,)), dma((2,)), dma((4,)), dma((4,)), dma((4,)), dma((4,)), dma((4,)), dma((4,))]
+    sems = [dma((17,)), dma((2,)), dma((2,))] + [dma((8,))] * 6
     sems += [dma((8,))] * 20 + [dma((16,))] * 4
     far = [
         pltpu.with_memory_space_constraint(a, pltpu.HBM)
@@ -396,13 +414,13 @@
             vmem((512, 256), BF16), vmem((512, 256), BF16),
             vmem((512, 256), BF16), vmem((512, 256), BF16),
             vmem((WIDTH_ROWS, 256), F32), vmem((WIDTH_ROWS, 256), F32),
-            vmem((8, 256), F32), vmem((8, 256), F32),
-            vmem((2, 256, 256), BF16), vmem((X, 64, 512), F32), vmem((X, 64, 512), BF16),
-            vmem((X, 64, 512), BF16), vmem((C, X, 64, 512), BF16), vmem((512, 256), BF16),
+            vmem((Y, 2, 8, 128), F32), vmem((Z, 2, 8, 128), F32),
+            vmem((2, 256, 256), BF16), vmem((2, X, 32, 512), F32), vmem((2, X, 32, 512), BF16),
+            vmem((2, X, 32, 512), BF16), vmem((C, X, 2, 32, 512), BF16), vmem((512, 256), BF16),
             vmem((Z, Y, 8, 128), BF16), vmem((Y, Z, 8, 128), BF16),
             vmem((Z, Y, 8, 128), BF16), vmem((Y, Z, 8, 128), BF16),
             vmem((Y, 8, 128), F32), vmem((Z, 8, 128), F32),
-            vmem((Y, 8, 128), F32), vmem((Z, 8, 128), F32),
+            vmem((Y, Y, 8, 128), BF16), vmem((Z, Z, 8, 128), BF16),
             vmem((Z, Y, WIDTH_ROWS, 256), BF16), vmem((Z, Y, WIDTH_ROWS, 256), BF16),
         ]
         + sems,

time: 53.7 us -> 50.7 us (0.944)
  Pallas kernels: 52.4 us -> 49.8 us
    pallas_call x1, Pallas kernels: 50 us -> 47.3 us  [local(): pl.pallas_call(exchange_kernel, out_shape=[jax.ShapeDtypeStruct((Z, 256,...]
where the time goes in v5:
time: 50.7 us; the launch traced here: 50.6 us
  Pallas kernels  49.8 us (98%)
  between operations  0.77 us (2%)
    pallas_call x1, Pallas kernels, local(): pl.pallas_call(exchange_kernel, out_shape=[jax.ShapeDtypeStruct((Z, 256,...  47.3 us
    pallas_call x1, Pallas kernels, local(): pl.pallas_call(finish_kernel, out_shape=[own, own, small, small, small, s...  2.42 us

profile of v5, /device:TPU:6, one launch (start us, length us, event | category | flops | bytes accessed | tf_op | source)
XLA Modules:
  0.0 50.6 jit_solution(8902932274113142162)
XLA Ops:
  0.6 0.0 copy-start.7
  0.6 0.0 copy-start.6
  0.7 0.0 copy-start.5
  0.7 0.0 copy-start.4
  0.7 0.0 copy-start.2
  0.7 0.0 copy-start.1
  0.7 0.0 copy-start
  0.7 0.0 copy-start.3
  0.7 47.3 %exchange.1 = (f32[8,256,256]{2,1,0:T(8,128)S(1)}, f32[256,2048]{1,0:T(8,128)S(1)}, bf16[8,8,8,128]{3,2,1,0:T(8,128)(2,1)S(1)}, bf16[8,8,8,128]{3,2,1,0:T(8,128)(2,1)S(1)}, f32[8,256]{1,0:T(8,128)S(1)}) custom-call(bf16[512,256]{1,0:T(8,128)(2,1)} %inputs.1, bf16[512,256]{1,0:T(8,128)(2,1)} %ocot.1, bf16[512,256]{1,0:T(8,128)(2,1)} %vcot.1, ...), custom_call_target="tpu_custom_call" | custom-call | tf_op jit(solution)/shard_map/exchange/pallas_call | solution.py:399
  48.1 0.0 copy-done.7
  48.1 0.0 copy-done.6
  48.1 0.0 copy-done.5
  48.1 0.0 copy-done.4
  48.1 0.0 copy-done.2
  48.1 0.0 copy-done.1
  48.1 0.0 copy-done
  48.1 0.0 copy-done.3
  48.1 2.4 %finish.1 = (f32[32,256]{1,0:T(8,128)}, f32[32,256]{1,0:T(8,128)}, f32[4,256]{1,0:T(4,128)}, f32[4,256]{1,0:T(4,128)}, f32[4,256]{1,0:T(4,128)}, /*index=5*/f32[...) custom-call(bf16[8,8,8,128]{3,2,1,0:T(8,128)(2,1)S(1)} %get-tuple-element.21.da, ...), custom_call_target="tpu_custom_call" | custom-call | tf_op jit(solution)/shard_map/finish/pallas_call | solution.py:437
Async XLA Ops:
  0.6 47.4 %copy-start.7 = (f32[4,256]{1,0:T(4,128)S(1)}, f32[4,256]{1,0:T(4,128)}, u32[]{:S(2)}) copy-start(f32[4,256]{1,0:T(4,128)} %os_.3) | copy-start | bytes 12292
  0.6 47.4 %copy-start.6 = (f32[4,256]{1,0:T(4,128)S(1)}, f32[4,256]{1,0:T(4,128)}, u32[]{:S(2)}) copy-start(f32[4,256]{1,0:T(4,128)} %om.3) | copy-start | bytes 12292
  0.7 47.4 %copy-start.5 = (f32[4,256]{1,0:T(4,128)S(1)}, f32[4,256]{1,0:T(4,128)}, u32[]{:S(2)}) copy-start(f32[4,256]{1,0:T(4,128)} %vs.3) | copy-start | bytes 12292
  0.7 47.4 %copy-start.4 = (f32[4,256]{1,0:T(4,128)S(1)}, f32[4,256]{1,0:T(4,128)}, u32[]{:S(2)}) copy-start(f32[4,256]{1,0:T(4,128)} %vm.3) | copy-start | bytes 12292
  0.7 47.4 %copy-start.2 = (f32[32,256]{1,0:T(8,128)S(1)}, f32[32,256]{1,0:T(8,128)}, u32[]{:S(2)}) copy-start(f32[32,256]{1,0:T(8,128)} %vw.3) | copy-start | bytes 98308
  0.7 47.4 %copy-start.1 = (bf16[2048,256]{1,0:T(8,128)(2,1)S(1)}, bf16[2048,256]{1,0:T(8,128)(2,1)}, u32[]{:S(2)}) copy-start(bf16[2048,256]{1,0:T(8,128)(2,1)} %of.3) | copy-start | bytes 3145732
  0.7 47.4 %copy-start = (bf16[2048,256]{1,0:T(8,128)(2,1)S(1)}, bf16[2048,256]{1,0:T(8,128)(2,1)}, u32[]{:S(2)}) copy-start(bf16[2048,256]{1,0:T(8,128)(2,1)} %vf.3) | copy-start | bytes 3145732
  0.7 47.4 %copy-start.3 = (f32[256,32]{0,1:T(8,128)S(1)}, f32[256,32]{0,1:T(8,128)}, u32[]{:S(2)}) copy-start(f32[256,32]{0,1:T(8,128)} %param.25) | copy-start | bytes 98308

commit v6 on v5

--- a/solution.py
+++ b/solution.py
@@ -39,7 +39,7 @@
 def exchange_kernel(
     inputs, ocot, vcot, first, second, lambdas, gain, vf, of, vw, ow, vm, vs, om, os_,
     wv_f, wo_f, da, db, low_v,
-    in_v, oc_v, vc_v, fi_v, se_v, vf_v, of_v, vw_v, ow_v, ma, mb,
+    in_v, oc_v, vc_v, fi_v, se_v, vf_v, of_v, vw_v, ow_v, la_v, ga_v, ma, mb,
     pair, ax, sx, rx, pq, heads,
     la, lb, ra, rb, sa, sb, ra2, rb2, wv, wo,
     load_sem,
@@ -88,6 +88,8 @@
             ("vf", vf.at[chip_rows], vf_v),
             ("oc", ocot, oc_v),
             ("of", of.at[chip_rows], of_v),
+            ("la", lambdas, la_v),
+            ("ga", gain, ga_v),
             ("fi", first, fi_v),
             ("se", second, se_v),
             ("vc", vcot, vc_v),
@@ -180,13 +182,15 @@
     ring_step(1, 0)
     ring_step(1, 1)
 
+    loads["la"].wait()
+    loads["ga"].wait()
     loads["fi"].wait()
     loads["se"].wait()
     for h in range(2):
         cols = slice(h * HEAD, (h + 1) * HEAD)
-        difference = fi_v[:, cols].astype(F32) - lambdas[h] * se_v[:, cols].astype(F32)
+        difference = fi_v[:, cols].astype(F32) - la_v[h] * se_v[:, cols].astype(F32)
         mean = jnp.mean(difference * difference, axis=-1, keepdims=True)
-        heads[:, cols] = (difference * lax.rsqrt(mean + 1e-06) * gain[...]).astype(BF16)
+        heads[:, cols] = (difference * lax.rsqrt(mean + 1e-06) * ga_v[...]).astype(BF16)
 
     x_all, passed = {}, []
     for h in range(2):
@@ -243,18 +247,20 @@
     open_group(z)
     open_group(lax.rem(z + Z - 1, Z))
     open_group(lax.rem(z + 1, Z))
+    r2a, r2b = {}, {}
     sum_a = la[z].astype(F32)
-    sum_b = lb[y].astype(F32)
     for d in NEAR:
         r1a[d].wait_recv()
         sum_a += ra[lax.rem(z + Z - d, Z)].astype(F32)
+    ra2[y] = sum_a.astype(BF16)
+    for d in FAR:
+        r2a[d] = send(ra2.at[y], ra2.at[y], r2a_s.at[d], r2a_r.at[d], at_y(d))
+    sum_b = lb[y].astype(F32)
+    for d in NEAR:
         r1b[d].wait_recv()
         sum_b += rb[lax.rem(y + Y - d, Y)].astype(F32)
-    ra2[y] = sum_a.astype(BF16)
     rb2[z] = sum_b.astype(BF16)
-    r2a, r2b = {}, {}
-    for d in FAR:
-        r2a[d] = send(ra2.at[y], ra2.at[y], r2a_s.at[d], r2a_r.at[d], at_y(d))
+    for d in FAR:
         r2b[d] = send(rb2.at[z], rb2.at[z], r2b_s.at[d], r2b_r.at[d], at_z(d))
 
     ring_wait(3, 0)
@@ -386,7 +392,7 @@
     near = pl.BlockSpec(memory_space=pltpu.VMEM)
     dma = pltpu.SemaphoreType.DMA
     vmem = pltpu.VMEM
-    sems = [dma((17,)), dma((2,)), dma((2,))] + [dma((8,))] * 6
+    sems = [dma((19,)), dma((2,)), dma((2,))] + [dma((8,))] * 6
     sems += [dma((8,))] * 20 + [dma((16,))] * 4
     far = [
         pltpu.with_memory_space_constraint(a, pltpu.HBM)
@@ -406,14 +412,14 @@
             jax.ShapeDtypeStruct((8, 256), F32),
         ],
         in_specs=[hbm] * 5
-        + [pl.BlockSpec(memory_space=pltpu.SMEM), pl.BlockSpec(memory_space=pltpu.VMEM)]
-        + [hbm] * 8,
+        + [hbm] * 10,
         out_specs=[near] * 5,
         scratch_shapes=[
             vmem((512, 256), BF16), vmem((512, 256), BF16), vmem((512, 256), BF16),
             vmem((512, 256), BF16), vmem((512, 256), BF16),
             vmem((512, 256), BF16), vmem((512, 256), BF16),
             vmem((WIDTH_ROWS, 256), F32), vmem((WIDTH_ROWS, 256), F32),
+            pltpu.SMEM((2,), F32), vmem((1, HEAD), F32),
             vmem((Y, 2, 8, 128), F32), vmem((Z, 2, 8, 128), F32),
             vmem((2, 256, 256), BF16), vmem((2, X, 32, 512), F32), vmem((2, X, 32, 512), BF16),
             vmem((2, X, 32, 512), BF16), vmem((C, X, 2, 32, 512), BF16), vmem((512, 256), BF16),

time: 50.7 us -> 50.2 us (level)
  no operation moved by 1% of the time
where the time goes in v6:
time: 50.2 us; the launch traced here: 50.1 us
  Pallas kernels  49.3 us (98%)
  between operations  0.77 us (2%)
    pallas_call x1, Pallas kernels, local(): pl.pallas_call(exchange_kernel, out_shape=[jax.ShapeDtypeStruct((Z, 256,...  46.9 us
    pallas_call x1, Pallas kernels, local(): pl.pallas_call(finish_kernel, out_shape=[own, own, small, small, small, s...  2.42 us

profile of v6, /device:TPU:6, one launch (start us, length us, event | category | flops | bytes accessed | tf_op | source)
XLA Modules:
  0.0 50.1 jit_solution(15352440942833707225)
XLA Ops:
  0.6 0.0 copy-start.7
  0.6 0.0 copy-start.6
  0.7 0.0 copy-start.5
  0.7 0.0 copy-start.4
  0.7 0.0 copy-start.2
  0.7 0.0 copy-start.1
  0.7 0.0 copy-start
  0.7 0.0 copy-start.3
  0.7 46.9 %exchange.1 = (f32[8,256,256]{2,1,0:T(8,128)S(1)}, f32[256,2048]{1,0:T(8,128)S(1)}, bf16[8,8,8,128]{3,2,1,0:T(8,128)(2,1)S(1)}, bf16[8,8,8,128]{3,2,1,0:T(8,128)(2,1)S(1)}, f32[8,256]{1,0:T(8,128)S(1)}) custom-call(bf16[512,256]{1,0:T(8,128)(2,1)} %inputs.1, bf16[512,256]{1,0:T(8,128)(2,1)} %ocot.1, bf16[512,256]{1,0:T(8,128)(2,1)} %vcot.1, ...), custom_call_target="tpu_custom_call" | custom-call | tf_op jit(solution)/shard_map/exchange/pallas_call | solution.py:405
  47.6 0.0 copy-done.7
  47.6 0.0 copy-done.6
  47.7 0.0 copy-done.5
  47.7 0.0 copy-done.4
  47.7 0.0 copy-done.2
  47.7 0.0 copy-done.1
  47.7 0.0 copy-done
  47.7 0.0 copy-done.3
  47.7 2.4 %finish.1 = (f32[32,256]{1,0:T(8,128)}, f32[32,256]{1,0:T(8,128)}, f32[4,256]{1,0:T(4,128)}, f32[4,256]{1,0:T(4,128)}, f32[4,256]{1,0:T(4,128)}, /*index=5*/f32[...) custom-call(bf16[8,8,8,128]{3,2,1,0:T(8,128)(2,1)S(1)} %get-tuple-element.21.da, ...), custom_call_target="tpu_custom_call" | custom-call | tf_op jit(solution)/shard_map/finish/pallas_call | solution.py:443
Async XLA Ops:
  0.6 47.0 %copy-start.7 = (f32[4,256]{1,0:T(4,128)S(1)}, f32[4,256]{1,0:T(4,128)}, u32[]{:S(2)}) copy-start(f32[4,256]{1,0:T(4,128)} %os_.3) | copy-start | bytes 12292
  0.6 47.0 %copy-start.6 = (f32[4,256]{1,0:T(4,128)S(1)}, f32[4,256]{1,0:T(4,128)}, u32[]{:S(2)}) copy-start(f32[4,256]{1,0:T(4,128)} %om.3) | copy-start | bytes 12292
  0.7 47.0 %copy-start.5 = (f32[4,256]{1,0:T(4,128)S(1)}, f32[4,256]{1,0:T(4,128)}, u32[]{:S(2)}) copy-start(f32[4,256]{1,0:T(4,128)} %vs.3) | copy-start | bytes 12292
  0.7 47.0 %copy-start.4 = (f32[4,256]{1,0:T(4,128)S(1)}, f32[4,256]{1,0:T(4,128)}, u32[]{:S(2)}) copy-start(f32[4,256]{1,0:T(4,128)} %vm.3) | copy-start | bytes 12292
  0.7 47.0 %copy-start.2 = (f32[32,256]{1,0:T(8,128)S(1)}, f32[32,256]{1,0:T(8,128)}, u32[]{:S(2)}) copy-start(f32[32,256]{1,0:T(8,128)} %vw.3) | copy-start | bytes 98308
  0.7 47.0 %copy-start.1 = (bf16[2048,256]{1,0:T(8,128)(2,1)S(1)}, bf16[2048,256]{1,0:T(8,128)(2,1)}, u32[]{:S(2)}) copy-start(bf16[2048,256]{1,0:T(8,128)(2,1)} %of.3) | copy-start | bytes 3145732
  0.7 47.0 %copy-start = (bf16[2048,256]{1,0:T(8,128)(2,1)S(1)}, bf16[2048,256]{1,0:T(8,128)(2,1)}, u32[]{:S(2)}) copy-start(bf16[2048,256]{1,0:T(8,128)(2,1)} %vf.3) | copy-start | bytes 3145732
  0.7 47.0 %copy-start.3 = (f32[256,32]{0,1:T(8,128)S(1)}, f32[256,32]{0,1:T(8,128)}, u32[]{:S(2)}) copy-start(f32[256,32]{0,1:T(8,128)} %param.25) | copy-start | bytes 98308
